TPU v7x, 32 devices: a whole 2x2x4 slice. The times are simulated.
32 devices in a mesh: sp: 8 (over z, x), dp: 4 (over y, core).
Axes of the slice: x: 2, y: 2, z: 4, core: 2. Of those that a mesh axis runs over, the one named last changes fastest.
Arguments:
- resid: bfloat16 [4, 2048, 2048], P('dp', 'sp'), may hold values from -4 to 4
- query: bfloat16 [4, 2048, 2048], P('dp', 'sp'), may hold values from -6 to 6
- keys: bfloat16 [4, 2048, 512], P('dp', 'sp'), may hold values from -6 to 6
- values: bfloat16 [4, 2048, 512], P('dp', 'sp'), may hold values from -6 to 6
- q_gain: float32 [128], replicated, may hold values from 0.7 to 5
- k_gain: float32 [128], replicated, may hold values from 0.7 to 5
- out_weight: bfloat16 [2048, 2048], P('dp'), may hold values from -0.5 to 0.5
- norm_gain: float32 [2048], replicated, may hold values from 0.1 to 1.9
- route_ids: int32 [4, 2048, 2], P('dp', 'sp'), may hold values from 0 to 31, all different within a row; in each aligned block of 256 rows (0 to 255, 256 to 511, ..., all dimensions but the last counted through in order) at most 24 rows name the same one
- route_weight: float32 [4, 2048, 2], P('dp', 'sp'), may hold values from 0.2 to 1
- expert_gate: bfloat16 [32, 2048, 1024], P(('sp', 'dp')), may hold values from -0.125 to 0.125
- expert_up: bfloat16 [32, 2048, 1024], P(('sp', 'dp')), may hold values from -0.125 to 0.125
- expert_down: bfloat16 [32, 1024, 2048], P(('sp', 'dp')), may hold values from -0.1875 to 0.1875
Outputs:
- layer_out: bfloat16 [4, 2048, 2048], P('dp', 'sp')
Inputs may be any that keep to these rules, and one draw needn't show every extreme that they name: `route_ids`: each row names 2 different experts. In the rows of one device no expert is named more than 24 times, and in some devices some expert is named exactly 24 times.
All inputs are finite; a program needn't handle non-finite values.
Results may differ from a plain program's by a relative error of at most 0.0095.
The roundings to bfloat16 on the way count: a program that leaves them out, or rounds other values in their place, can miss the bound.
Values may be sent and summed in bfloat16 or wider, within the bound.
A program may use at most 128 MiB of HBM per device.

v0:
```python
import functools

import jax
import jax.numpy as jnp
from jax import lax
from jax.experimental import pallas as pl
from jax.experimental.pallas import tpu as pltpu
from jax.sharding import PartitionSpec as P

GRID_W = 64
EPSILON = 1e-06
THETA = 10000.0
LIMIT = 7.0
SLOPE = 1.702
LOG2E = 1.4426950408889634
MESH = pl.DeviceIdType.MESH
VMEM_BYTES = 64000000


def split_of(count, inner):
    return (count // inner, inner) if count % inner == 0 else (count, 1)


def turn_tables(places, head_dim):
    quarter = head_dim // 4
    inverse = THETA ** (-jnp.arange(quarter, dtype=jnp.float32) / quarter)
    row = (places // GRID_W).astype(jnp.float32)[:, None] * inverse[None, :]
    col = (places % GRID_W).astype(jnp.float32)[:, None] * inverse[None, :]
    cosine = jnp.concatenate([jnp.cos(row)] * 2 + [jnp.cos(col)] * 2, axis=-1)
    sine = jnp.concatenate(
        [-jnp.sin(row), jnp.sin(row), -jnp.sin(col), jnp.sin(col)], axis=-1
    )
    return cosine, sine


def attention_kernel(
    planes, lanes_x, outer_dp, inner_dp,
    q_ref, k_ref, v_ref, qg_ref, kg_ref, cos_ref, sin_ref, resid_ref, ng_ref, w_ref,
    upd_ref, normed_ref,
    kall, vall, wall, qt, acc, mx, ls, head_out,
    kx_s, kx_r, kz_s, kz_r, vz_s, vz_r, vx_s, vx_r, wy_s, wy_r, wc_s, wc_r, loc,
):
    Z, X, Y, C = planes, lanes_x, outer_dp, inner_dp
    rows, head_dim = cos_ref.shape
    q_heads = q_ref.shape[1] // head_dim
    kv_heads = k_ref.shape[1] // head_dim
    group = q_heads // kv_heads
    w_rows = w_ref.shape[0]
    sp, dp = lax.axis_index("sp"), lax.axis_index("dp")
    z, x = sp // X, sp % X
    y, c = dp // C, dp % C
    up_ok, down_ok = z + 1 < Z, z > 0

    barrier = pltpu.get_barrier_semaphore()

    def greet(device):
        pl.semaphore_signal(barrier, inc=1, device_id=device, device_id_type=MESH)

    for j in range(1, X):
        greet((z * X + (x + j) % X, dp))

    @pl.when(up_ok)
    def _():
        greet((sp + X, dp))

    @pl.when(down_ok)
    def _():
        greet((sp - X, dp))

    for j in range(1, Y):
        greet((sp, ((y + j) % Y) * C + c))
    for j in range(1, C):
        greet((sp, y * C + (c + j) % C))

    def krows(block):
        return pl.ds(pl.multiple_of(block * rows, rows), rows)

    def wrows(block):
        return pl.ds(pl.multiple_of(block * w_rows, w_rows), w_rows)

    v_own = pltpu.make_async_copy(v_ref, vall.at[krows(sp)], loc.at[0])
    v_own.start()
    w_own = pltpu.make_async_copy(w_ref, wall.at[wrows(dp)], loc.at[1])
    w_own.start()

    lane = lax.broadcasted_iota(jnp.int32, (rows, head_dim), 1)
    first = lane % (head_dim // 2) < head_dim // 4

    def turned(value, gain):
        value = value.astype(jnp.float32)
        value = value * lax.rsqrt(jnp.mean(value * value, axis=-1, keepdims=True) + EPSILON) * gain
        swapped = jnp.where(
            first,
            pltpu.roll(value, head_dim - head_dim // 4, 1),
            pltpu.roll(value, head_dim // 4, 1),
        )
        return (value * cos_ref[...] + swapped * sin_ref[...]).astype(jnp.bfloat16)

    for g in range(kv_heads):
        span = slice(g * head_dim, (g + 1) * head_dim)
        kall[krows(sp), span] = turned(k_ref[:, span], kg_ref[...])

    count = (X - 1) + (Y - 1) + (C - 1) + up_ok.astype(jnp.int32) + down_ok.astype(jnp.int32)
    v_own.wait()
    w_own.wait()
    pl.semaphore_wait(barrier, count)

    def remote(buf, sl, ssem, rsem, device):
        return pltpu.make_async_remote_copy(
            src_ref=buf.at[sl], dst_ref=buf.at[sl], send_sem=ssem, recv_sem=rsem,
            device_id=device, device_id_type=MESH,
        )

    def kx(j):
        return remote(kall, krows(sp), kx_s.at[j], kx_r.at[j], (z * X + (x + j) % X, dp))

    def kz(d, s, j):
        plane = z - s if d == 0 else z + s
        device = (sp + X if d == 0 else sp - X, dp)
        at = (d * (Z - 1) + s) * X + j
        return remote(kall, krows(plane * X + (x + X - j) % X), kz_s.at[at], kz_r.at[at], device)

    def vz(d, s):
        plane = z - s if d == 0 else z + s
        device = (sp + X if d == 0 else sp - X, dp)
        at = d * (Z - 1) + s
        return remote(vall, krows(plane * X + x), vz_s.at[at], vz_r.at[at], device)

    def vx(slot, plane, j):
        at = slot * X + j
        return remote(
            vall, krows(plane * X + x), vx_s.at[at], vx_r.at[at], (z * X + (x + j) % X, dp)
        )

    def sends(d, s):
        if d == 0:
            return jnp.logical_and(up_ok, z - s >= 0)
        return jnp.logical_and(down_ok, z + s < Z)

    def gets(d, s):
        return z - s - 1 >= 0 if d == 0 else z + s + 1 < Z

    def wy(j):
        return remote(wall, wrows(dp), wy_s.at[j], wy_r.at[j], (sp, ((y + j) % Y) * C + c))

    def wc(j, i):
        at = j * C + i
        return remote(
            wall, wrows(((y + Y - j) % Y) * C + c), wc_s.at[at], wc_r.at[at],
            (sp, y * C + (c + i) % C),
        )

    for j in range(1, X):
        kx(j).start()
    for d in range(2):
        @pl.when(sends(d, 0))
        def _(d=d):
            kz(d, 0, 0).start()
            vz(d, 0).start()
    for j in range(1, X):
        vx(0, z, j).start()
    for j in range(1, Y):
        wy(j).start()
    for i in range(1, C):
        wc(0, i).start()

    def prepare_queries(h, carry):
        at = pl.ds(pl.multiple_of(h * head_dim, head_dim), head_dim)
        qt[h] = turned(q_ref[:, at], qg_ref[...])
        return carry

    lax.fori_loop(0, q_heads // 4, prepare_queries, 0)
    for j in range(1, X):
        kx(j).wait_recv()
    for d in range(2):
        @pl.when(sends(d, 0))
        def _(d=d):
            for j in range(1, X):
                kz(d, 0, j).start()
    lax.fori_loop(q_heads // 4, q_heads, prepare_queries, 0)

    factor = head_dim ** (-0.5) * LOG2E
    keys_in = X * rows

    def attend(plane, fresh):
        at_rows = pl.ds(pl.multiple_of(plane * keys_in, keys_in), keys_in)

        def one_group(i, carry):
            span = pl.ds(pl.multiple_of(i * head_dim, head_dim), head_dim)
            for u in range(group):
                h = i * group + u
                scores = lax.dot_general(
                    qt[h], kall[at_rows, span], (((1,), (1,)), ((), ())),
                    preferred_element_type=jnp.float32,
                )
                top = jnp.max(scores, axis=-1, keepdims=True)
                if not fresh:
                    before = mx[h]
                    top = jnp.maximum(before[:, :1], top)
                lifted = jnp.exp2((scores - top) * factor)
                total = jnp.sum(lifted, axis=-1, keepdims=True)
                part = jnp.dot(
                    lifted.astype(jnp.bfloat16), vall[at_rows, span],
                    preferred_element_type=jnp.float32,
                )
                wide = jnp.broadcast_to(top, (rows, head_dim))
                wide_total = jnp.broadcast_to(total, (rows, head_dim))
                if fresh:
                    acc[h], ls[h] = part, wide_total
                else:
                    fade = jnp.exp2((before - wide) * factor)
                    acc[h] = acc[h] * fade + part
                    ls[h] = ls[h] * fade + wide_total
                mx[h] = wide
            return carry

        lax.fori_loop(0, kv_heads, one_group, 0)

    def wait_vx(slot, plane):
        for j in range(1, X):
            vx(slot, plane, j).wait_recv()

    def attend_step(s):
        def one(t, carry):
            plane = jnp.where(t == 0, z - s - 1, z + s + 1)

            @pl.when(jnp.logical_and(plane >= 0, plane < Z))
            def _():
                wait_vx(1 + s + t * (Z - 1), plane)
                attend(plane, False)
            return carry

        lax.fori_loop(0, 2, one, 0)

    for s in range(Z - 1):
        for d in range(2):
            @pl.when(gets(d, s))
            def _(d=d, s=s):
                plane = z - s - 1 if d == 0 else z + s + 1
                vz(d, s).wait_recv()
                for j in range(1, X):
                    vx(1 + s + d * (Z - 1), plane, j).start()
                if s + 1 < Z - 1:
                    @pl.when(sends(d, s + 1))
                    def _():
                        vz(d, s + 1).start()
                for j in range(X):
                    kz(d, s, j).wait_recv()
                    if s + 1 < Z - 1:
                        @pl.when(sends(d, s + 1))
                        def _(j=j):
                            kz(d, s + 1, j).start()
        if s == 0:
            wait_vx(0, z)
            attend(z, True)
        else:
            attend_step(s - 1)

    for j in range(1, Y):
        wy(j).wait_recv()
        for i in range(1, C):
            wc(j, i).start()
    if Z == 1:
        wait_vx(0, z)
        attend(z, True)
    else:
        attend_step(Z - 2)

    for h in range(q_heads):
        head_out[:, h * head_dim:(h + 1) * head_dim] = (acc[h] / ls[h]).astype(jnp.bfloat16)

    for j in range(Y):
        for i in range(1, C):
            wc(j, i).wait_recv()

    width = wall.shape[1]
    tile = min(256, width)

    def project(n, total):
        at = pl.ds(pl.multiple_of(n * tile, tile), tile)
        projected = jnp.dot(head_out[...], wall[:, at], preferred_element_type=jnp.float32)
        updated = (resid_ref[:, at].astype(jnp.float32) + projected).astype(jnp.bfloat16)
        upd_ref[:, at] = updated
        wide = updated.astype(jnp.float32)
        return total + jnp.sum(wide * wide, axis=-1, keepdims=True)

    square = lax.fori_loop(0, width // tile, project, jnp.zeros((rows, 1), jnp.float32))
    scale = lax.rsqrt(square / width + EPSILON)

    def normalize(n, carry):
        at = pl.ds(pl.multiple_of(n * tile, tile), tile)
        normed_ref[:, at] = (
            upd_ref[:, at].astype(jnp.float32) * scale * ng_ref[:, at]
        ).astype(jnp.bfloat16)
        return carry

    lax.fori_loop(0, width // tile, normalize, 0)

    for j in range(1, X):
        kx(j).wait_send()
        vx(0, z, j).wait_send()
    for d in range(2):
        for s in range(Z - 1):
            @pl.when(sends(d, s))
            def _(d=d, s=s):
                vz(d, s).wait_send()
                for j in range(X):
                    kz(d, s, j).wait_send()

            @pl.when(gets(d, s))
            def _(d=d, s=s):
                plane = z - s - 1 if d == 0 else z + s + 1
                for j in range(1, X):
                    vx(1 + s + d * (Z - 1), plane, j).wait_send()
    for j in range(1, Y):
        wy(j).wait_send()
    for j in range(Y):
        for i in range(1, C):
            wc(j, i).wait_send()


def attention(query, keys, values, q_gain, k_gain, cosine, sine, resid, norm_gain, out_weight):
    sp_count, dp_count = lax.axis_size("sp"), lax.axis_size("dp")
    planes = 4 if sp_count % 4 == 0 else 1
    lanes_x = sp_count // planes
    outer_dp, inner_dp = split_of(dp_count, 2)
    rows, head_dim = cosine.shape
    q_heads = query.shape[1] // head_dim
    width = resid.shape[1]
    dma = pltpu.SemaphoreType.DMA
    vmem = pl.BlockSpec(memory_space=pltpu.VMEM)
    hops = 2 * max(planes - 1, 1)
    full_kv = (sp_count * rows, keys.shape[1])
    return pl.pallas_call(
        functools.partial(attention_kernel, planes, lanes_x, outer_dp, inner_dp),
        name="gathered_attention",
        out_shape=(
            jax.ShapeDtypeStruct((rows, width), jnp.bfloat16),
            jax.ShapeDtypeStruct((rows, width), jnp.bfloat16),
        ),
        in_specs=[vmem, vmem, pl.BlockSpec(memory_space=pl.ANY)]
        + [vmem] * 6
        + [pl.BlockSpec(memory_space=pl.ANY)],
        out_specs=(vmem, vmem),
        scratch_shapes=[
            pltpu.VMEM(full_kv, jnp.bfloat16),
            pltpu.VMEM(full_kv, jnp.bfloat16),
            pltpu.VMEM((dp_count * out_weight.shape[0], width), jnp.bfloat16),
            pltpu.VMEM((q_heads, rows, head_dim), jnp.bfloat16),
            pltpu.VMEM((q_heads, rows, head_dim), jnp.float32),
            pltpu.VMEM((q_heads, rows, head_dim), jnp.float32),
            pltpu.VMEM((q_heads, rows, head_dim), jnp.float32),
            pltpu.VMEM((rows, q_heads * head_dim), jnp.bfloat16),
            dma((lanes_x,)), dma((lanes_x,)),
            dma((hops * lanes_x,)), dma((hops * lanes_x,)),
            dma((hops,)), dma((hops,)),
            dma(((hops + 1) * lanes_x,)), dma(((hops + 1) * lanes_x,)),
            dma((outer_dp,)), dma((outer_dp,)),
            dma((outer_dp * inner_dp,)), dma((outer_dp * inner_dp,)),
            dma((2,)),
        ],
        compiler_params=pltpu.CompilerParams(
            collective_id=0, has_side_effects=True, vmem_limit_bytes=VMEM_BYTES
        ),
    )(
        query, keys, values, q_gain[None], k_gain[None], cosine, sine, resid,
        norm_gain[None], out_weight,
    )


def apply_expert(batch, gate_matrix, up_matrix, down_matrix):
    flat_rows = batch.reshape(-1, batch.shape[-1])
    gated = jnp.minimum(jnp.dot(flat_rows, gate_matrix, preferred_element_type=jnp.float32), LIMIT)
    linear = jnp.clip(
        jnp.dot(flat_rows, up_matrix, preferred_element_type=jnp.float32), -LIMIT, LIMIT
    )
    active = (gated * jax.nn.sigmoid(SLOPE * gated) * (linear + 1.0)).astype(jnp.bfloat16)
    return (
        jnp.dot(active, down_matrix, preferred_element_type=jnp.float32)
        .astype(jnp.bfloat16)
        .reshape(batch.shape)
    )


def per_device(
    resid,
    query,
    keys,
    values,
    q_gain,
    k_gain,
    out_weight,
    norm_gain,
    route_ids,
    route_weight,
    expert_gate,
    expert_up,
    expert_down,
):
    span_devices = lax.axis_size("sp")
    experts_total = span_devices * lax.axis_size("dp")
    tok_rows = resid.shape[1]
    model_width = resid.shape[2]
    head_dim = q_gain.shape[0]
    places = lax.axis_index("sp") * tok_rows + jnp.arange(tok_rows, dtype=jnp.int32)
    cosine, sine = turn_tables(places, head_dim)
    updated, normed = attention(
        query[0], keys[0], values[0], q_gain, k_gain, cosine, sine, resid[0], norm_gain, out_weight
    )
    widened = updated.astype(jnp.float32)
    top_count = route_ids.shape[2]
    capacity = max(2, 3 * tok_rows * top_count // (2 * experts_total))
    chosen = route_ids[0].reshape(-1)
    onehot = (chosen[:, None] == jnp.arange(experts_total, dtype=jnp.int32)[None, :]).astype(
        jnp.int32
    )
    earlier = jnp.sum((jnp.cumsum(onehot, axis=0) - onehot) * onehot, axis=1)
    target = chosen * capacity + earlier
    sources = jnp.arange(tok_rows * top_count, dtype=jnp.int32) // top_count
    slot_table = jnp.full((experts_total * capacity,), tok_rows, jnp.int32).at[target].set(sources)
    padded = jnp.concatenate([normed, jnp.zeros((1, model_width), jnp.bfloat16)], axis=0)
    outgoing = padded[slot_table].reshape(experts_total, capacity, model_width)
    answered = apply_expert(
        lax.all_to_all(outgoing, ("sp", "dp"), split_axis=0, concat_axis=0, tiled=True),
        expert_gate[0],
        expert_up[0],
        expert_down[0],
    )
    returned = lax.all_to_all(answered, ("sp", "dp"), split_axis=0, concat_axis=0, tiled=True)
    rows_back = returned.reshape(experts_total * capacity, model_width)
    slots = target.reshape(tok_rows, top_count)
    combined = sum(
        rows_back[slots[:, i]].astype(jnp.float32) * route_weight[0, :, i][:, None]
        for i in range(top_count)
    )
    return (widened + combined).astype(jnp.bfloat16)[None]


def solution(mesh):
    placed = (
        P("dp", "sp", None),
        P("dp", "sp", None),
        P("dp", "sp", None),
        P("dp", "sp", None),
        P(),
        P(),
        P("dp", None),
        P(),
        P("dp", "sp", None),
        P("dp", "sp", None),
        P(("sp", "dp"), None, None),
        P(("sp", "dp"), None, None),
        P(("sp", "dp"), None, None),
    )
    return jax.shard_map(
        per_device, mesh=mesh, in_specs=placed, out_specs=P("dp", "sp", None), check_vma=False
    )
```

profile of v0, /device:TPU:0, one launch (start us, length us, event | category | flops | bytes accessed | tf_op | source)
XLA Modules:
  0.0 264.9 jit_solution(15097267421758312239)
XLA Ops:
  0.0 0.8 copy.24
  0.8 0.1 eq.31
  1.0 0.1 eq.27
  1.2 1.2 reduce-window.6
  2.4 0.2 slice_reduce_fusion
  2.6 0.1 mul.92
  2.8 0.1 fusion.16
  2.9 2.4 scatter_custom_fusion
  5.4 1.0 fusion.18
  6.4 0.8 pad_maximum_fusion.cos_ref
  7.2 0.8 pad_maximum_fusion.1.sin_ref
  8.0 79.6 %gathered_attention.1 = (bf16[256,2048]{1,0:T(8,128)(2,1)}, bf16[256,2048]{1,0:T(8,128)(2,1)}) custom-call(bf16[256,2048]{1,0:T(8,128)(2,1)} %bitcast.61, bf16[256,512]{1,0:T(8,128)(2,1)} %bitcast.63, bf16[256,512]{1,0:T(8,128)(2,1)} %bitcast.64, f32[1,128]{1,0:T(1,128)} %bitcast.70, f32[1,128]{1,0:T(1,128)} %bitcast.71, ...), custom_call_target="tpu_custom_call" | custom-call | tf_op jit(solution)/shard_map/gathered_attention/pallas_call | solution.py:334
  87.6 1.3 concatenate.11
  88.9 4.3 %gather_fusion = bf16[768,2048]{1,0:T(8,128)(2,1)} fusion(bf16[257,2048]{1,0:T(8,128)(2,1)S(1)} %concatenate.11, s32[1024]{0:T(1024)S(1)} %pad_clamp_fusion.2), kind=kCustom, calls=%fused_computation | custom fusion | bytes 6294528 | tf_op jit(solution)/shard_map/gather | solution.py:422
  93.2 0.0 copy-start.1
  93.2 75.9 %all_to_all.10 = bf16[32,24,2048]{2,1,0:T(8,128)(2,1)S(1)} all-to-all(bf16[32,24,2048]{2,1,0:T(8,128)(2,1)} %bitcast.57), channel_id=1, replica_groups=mesh['sp'=8,'dp'=4] {'sp','dp'}, dimensions={0} | all-to-all | bytes 6291456 | tf_op jit(solution)/shard_map/all_to_all | solution.py:424
  169.1 0.0 copy-done.1
  169.1 0.0 copy-start.2
  169.1 3.4 %fusion.2 = f32[768,1024]{1,0:T(8,128)S(1)} fusion(bf16[768,2048]{1,0:T(8,128)(2,1)S(1)} %bitcast.59, bf16[1,2048,1024]{2,1,0:T(8,128)(2,1)S(1)} %copy-done.1), kind=kOutput, calls=%fused_computation.6 | convolution fusion | flops 3221225472 | bytes 10485760 | tf_op jit(solution)/shard_map/dot_general | solution.py:375
  172.5 0.0 copy-done.2
  172.5 0.0 copy-start.3
  172.5 4.1 %multiply_convert_fusion = bf16[768,1024]{1,0:T(8,128)(2,1)S(1)} fusion(f32[768,1024]{1,0:T(8,128)S(1)} %fusion.2, bf16[768,2048]{1,0:T(8,128)(2,1)S(1)} %bitcast.60, bf16[1,2048,1024]{2,1,0:T(8,128)(2,1)S(1)} %copy-done.2), kind=kOutput, calls=%fused_computation.11 | convolution fusion | flops 3229089792 | bytes 12058624 | tf_op jit(solution)/shard_map/dot_general | solution.py:373
  176.7 0.0 copy-done.3
  176.7 4.8 %fusion.6 = bf16[768,2048]{1,0:T(8,128)(2,1)} fusion(bf16[768,1024]{1,0:T(8,128)(2,1)S(1)} %multiply_convert_fusion, bf16[1,1024,2048]{2,1,0:T(8,128)(2,1)S(1)} %copy-done.3), kind=kOutput, calls=%fused_computation.10 | convolution fusion | flops 3222798336 | bytes 8912896 | tf_op jit(solution)/shard_map/dot_general | solution.py:379
  181.5 0.0 copy-start
  181.5 3.7 %all-to-all-start.1 = ((bf16[32,24,2048]{2,1,0:T(8,128)(2,1)}), bf16[32,24,2048]{2,1,0:T(8,128)(2,1)S(1)}, u32[]{:S(2)}, u32[]{:S(2)}) async-start(bf16[32,24,2048]{2,1,0:T(8,128)(2,1)} %bitcast.58), calls=%async_computation.1 | async-start | bytes 6291456 | tf_op jit(solution)/shard_map/all_to_all | solution.py:429
  185.2 0.1 reduce_sum.15
  185.3 0.2 fusion.12
  185.6 0.0 copy-done
  185.6 71.2 %all-to-all-done.1 = bf16[32,24,2048]{2,1,0:T(8,128)(2,1)S(1)} async-done(((bf16[32,24,2048]{2,1,0:T(8,128)(2,1)}), bf16[32,24,2048]{2,1,0:T(8,128)(2,1)S(1)}, u32[]{:S(2)}, u32[]{:S(2)}) %all-to-all-start.1) | async-done | bytes 3145760 | tf_op jit(solution)/shard_map/all_to_all | solution.py:429
  256.8 2.3 gather_fusion.2
  259.1 2.3 gather_fusion.1
  261.5 3.4 %fusion.11 = bf16[1,256,2048]{2,1,0:T(8,128)(2,1)} fusion(bf16[256,2048]{1,0:T(8,128)(2,1)} %gather_fusion.2, bf16[256,2048]{1,0:T(8,128)(2,1)} %gather_fusion.1, bf16[256,2048]{1,0:T(8,128)(2,1)} %get-tuple-element.7, f32[256]{0:T(256)S(1)} %bitcast.68, f32[256]{0:T(256)S(1)} %bitcast.67), kind=kLoop, calls=%fused_computation.13 | loop fusion | flops 4194304 | bytes 4196352 | tf_op jit(solution)/shard_map/broadcast_in_dim | solution.py:436
  (13 shorter events, 0.1 us)
Async XLA Ops:
  93.2 75.9 %copy-start.1 = (bf16[1,2048,1024]{2,1,0:T(8,128)(2,1)S(1)}, bf16[1,2048,1024]{2,1,0:T(8,128)(2,1)}, u32[]{:S(2)}) copy-start(bf16[1,2048,1024]{2,1,0:T(8,128)(2,1)} %param.24) | copy-start | bytes 12582916
  169.1 3.5 %copy-start.2 = (bf16[1,2048,1024]{2,1,0:T(8,128)(2,1)S(1)}, bf16[1,2048,1024]{2,1,0:T(8,128)(2,1)}, u32[]{:S(2)}) copy-start(bf16[1,2048,1024]{2,1,0:T(8,128)(2,1)} %param.23) | copy-start | bytes 12582916
  172.5 4.2 %copy-start.3 = (bf16[1,1024,2048]{2,1,0:T(8,128)(2,1)S(1)}, bf16[1,1024,2048]{2,1,0:T(8,128)(2,1)}, u32[]{:S(2)}) copy-start(bf16[1,1024,2048]{2,1,0:T(8,128)(2,1)} %param.25) | copy-start | bytes 12582916
  181.5 4.1 %copy-start = (f32[1,256,2]{1,2,0:T(2,128)S(1)}, f32[1,256,2]{1,2,0:T(2,128)}, u32[]{:S(2)}) copy-start(f32[1,256,2]{1,2,0:T(2,128)} %param.22) | copy-start | bytes 6148
  181.5 75.3 %all-to-all-start.1 = ((bf16[32,24,2048]{2,1,0:T(8,128)(2,1)}), bf16[32,24,2048]{2,1,0:T(8,128)(2,1)S(1)}, u32[]{:S(2)}, u32[]{:S(2)}) async-start(bf16[32,24,2048]{2,1,0:T(8,128)(2,1)} %bitcast.58), calls=%async_computation.1 | async-start | bytes 6291456 | tf_op jit(solution)/shard_map/all_to_all | solution.py:429
where the time goes:
time: 265 us
  Pallas kernels  79.6 us (30%)
  blocking collectives  75.9 us (29%)
  waiting for transfers between devices  71.2 us (27%)
  local copies, waits for them, and re-layouts  14.3 us (5%)
  matrix products  12.4 us (5%)
  other arithmetic  7.64 us (3%)
  starting transfers between devices  3.66 us (1%)
    pallas_call x1, Pallas kernels, attention(): pl.pallas_call(functools.partial(attention_kernel, planes, lanes_x, outer...  79.6 us
    all_to_all x1, blocking collectives, per_device(): lax.all_to_all(outgoing, ('sp', 'dp'), split_axis=0, concat_axis=0, tiled...  75.9 us
    all_to_all x1, waiting for transfers between devices, per_device(): lax.all_to_all(answered, ('sp', 'dp'), split_axis=0, concat_axis=0, tiled...  71.2 us
  transfers between devices with their start and end apart: 1, of which 1 were waited for; matrix products, arithmetic and copies ran while one was open for 0% of the time, Pallas kernels for 0%

commit v1 on v0

--- a/solution.py
+++ b/solution.py
@@ -15,6 +15,7 @@
 LOG2E = 1.4426950408889634
 MESH = pl.DeviceIdType.MESH
 VMEM_BYTES = 64000000
+CHUNKS = 4
 
 
 def split_of(count, inner):
@@ -368,18 +369,458 @@
     )
 
 
-def apply_expert(batch, gate_matrix, up_matrix, down_matrix):
-    flat_rows = batch.reshape(-1, batch.shape[-1])
-    gated = jnp.minimum(jnp.dot(flat_rows, gate_matrix, preferred_element_type=jnp.float32), LIMIT)
-    linear = jnp.clip(
-        jnp.dot(flat_rows, up_matrix, preferred_element_type=jnp.float32), -LIMIT, LIMIT
-    )
-    active = (gated * jax.nn.sigmoid(SLOPE * gated) * (linear + 1.0)).astype(jnp.bfloat16)
-    return (
-        jnp.dot(active, down_matrix, preferred_element_type=jnp.float32)
-        .astype(jnp.bfloat16)
-        .reshape(batch.shape)
-    )
+def experts_kernel(
+    planes, lanes_x, slots,
+    meta_ref, normed_ref, upd_ref, gate_hbm, up_hbm, down_hbm,
+    out_ref,
+    meta, raw, pk, epk, xb, rb, fr, fp, ptab, whi, wlo, tri, xs, act, acc, gate_w, up_w, down_w,
+    meta_s, meta_r, zs, zr, es, er, rs, rr, fs, fa, loc,
+):
+    Z, X, K = planes, lanes_x, slots
+    rows, width = normed_ref.shape
+    DP = lax.axis_size("dp")
+    EP = X * DP
+    S = EP * K
+    top = meta_ref.shape[0] // 2
+    chunks = zr.shape[1]
+    part = width // chunks
+    hidden = gate_w.shape[1]
+    sp, dp = lax.axis_index("sp"), lax.axis_index("dp")
+    z, x = sp // X, sp % X
+    p = x * DP + dp
+    f32, bf16 = jnp.float32, jnp.bfloat16
+
+    def cols(ck):
+        return pl.ds(pl.multiple_of(ck * part, part), part)
+
+    def peer(q):
+        return (z * X + q // DP, q % DP)
+
+    def loop(low, high, body):
+        def step(i, carry):
+            body(i)
+            return carry
+        lax.fori_loop(low, high, step, 0)
+
+    def remote(src, dst, ssem, rsem, device):
+        return pltpu.make_async_remote_copy(
+            src_ref=src, dst_ref=dst, send_sem=ssem, recv_sem=rsem,
+            device_id=device, device_id_type=MESH,
+        )
+
+    weights = [
+        pltpu.make_async_copy(gate_hbm, gate_w, loc.at[0]),
+        pltpu.make_async_copy(up_hbm, up_w, loc.at[1]),
+        pltpu.make_async_copy(down_hbm, down_w, loc.at[2]),
+    ]
+
+    barrier = pltpu.get_barrier_semaphore()
+
+    def greet(device):
+        pl.semaphore_signal(barrier, inc=1, device_id=device, device_id_type=MESH)
+
+    loop(1, EP, lambda j: greet(peer((p + j) % EP)))
+    for j in range(1, Z):
+        greet((((z + j) % Z) * X + x, dp))
+    for copy in weights:
+        copy.start()
+    tri[...] = (
+        lax.broadcasted_iota(jnp.int32, (rows, rows), 0)
+        < lax.broadcasted_iota(jnp.int32, (rows, rows), 1)
+    ).astype(f32).astype(bf16)
+    pl.semaphore_wait(barrier, EP - 1 + Z - 1)
+
+    def side(d):
+        return (sp + X if d == 0 else sp - X, dp)
+
+    def exists(d):
+        return z + 1 < Z if d == 0 else z >= 1
+
+    def at_end(d):
+        return z == Z - 1 if d == 0 else z == 0
+
+    def next_end(d):
+        return z + 1 == Z - 1 if d == 0 else z - 1 == 0
+
+    def end_of(d):
+        return Z - 1 if d == 0 else 0
+
+    def meta_copy(j):
+        return remote(
+            meta_ref, meta.at[z], meta_s.at[j], meta_r.at[z], (((z + j) % Z) * X + x, dp)
+        )
+
+    def own_raw(d, ck):
+        return remote(
+            normed_ref.at[:, cols(ck)], raw.at[z, :, cols(ck)],
+            zs.at[z if d == 0 else Z, ck], zr.at[z, ck], side(d),
+        )
+
+    def raw_on(d, src, ck):
+        return remote(
+            raw.at[src, :, cols(ck)], raw.at[src, :, cols(ck)],
+            zs.at[src, ck], zr.at[src, ck], side(d),
+        )
+
+    def packed_on(d, src, slot, ck):
+        return remote(
+            epk.at[slot, :, :, cols(ck)], pk.at[src, :, :, cols(ck)],
+            zs.at[slot, ck], zr.at[src, ck], side(d),
+        )
+
+    def landed(buf, index, sem):
+        view = buf.at[index]
+        pltpu.make_async_copy(view, view, sem).wait()
+
+    def spread(src, ck):
+        pltpu.make_async_copy(
+            pk.at[src, p, :, cols(ck)], xb.at[src, p, :, cols(ck)], er.at[src, ck]
+        ).start()
+
+        def one(j):
+            q = (p + j) % EP
+            remote(
+                pk.at[src, q, :, cols(ck)], xb.at[src, p, :, cols(ck)],
+                es.at[src, ck], er.at[src, ck], peer(q),
+            ).start()
+
+        loop(1, EP, one)
+
+    def give_back(src, ck):
+        pltpu.make_async_copy(
+            xb.at[src, p, :, cols(ck)], rb.at[src, p, :, cols(ck)], rr.at[src, ck]
+        ).start()
+
+        def one(j):
+            q = (p + j) % EP
+            remote(
+                xb.at[src, q, :, cols(ck)], rb.at[src, p, :, cols(ck)],
+                rs.at[src, ck], rr.at[src, ck], peer(q),
+            ).start()
+
+        loop(1, EP, one)
+
+    def build(src, plane, index):
+        info = meta[src]
+        lane_expert = lax.broadcasted_iota(jnp.int32, (EP, rows), 0).astype(f32) + (
+            plane * EP
+        ).astype(f32) if not isinstance(plane, int) else (
+            lax.broadcasted_iota(jnp.int32, (EP, rows), 0).astype(f32) + float(plane * EP)
+        )
+        named = jnp.zeros((EP, rows), f32)
+        scale = jnp.zeros((EP, rows), f32)
+        for i in range(top):
+            hit = info[i:i + 1] == lane_expert
+            named = jnp.where(hit, 1.0, named)
+            scale = jnp.where(hit, info[top + i:top + i + 1], scale)
+        rank = jnp.dot(named.astype(bf16), tri[...], preferred_element_type=f32)
+        rank = jnp.where(named > 0.0, rank, -1.0)
+        place = lax.broadcasted_iota(jnp.int32, (K, rows), 0).astype(f32)
+        ones, scaled = [], []
+        for e in range(EP):
+            one = jnp.where(rank[e:e + 1] == place, 1.0, 0.0)
+            ones.append(one)
+            scaled.append(one * scale[e:e + 1])
+        ptab[index] = jnp.concatenate(ones, axis=0).astype(bf16)
+        spare = whi.shape[2] - S
+        if spare:
+            scaled.append(jnp.zeros((spare, rows), f32))
+        turned = jnp.concatenate(scaled, axis=0).T
+        high = turned.astype(bf16)
+        whi[index] = high
+        wlo[index] = (turned - high.astype(f32)).astype(bf16)
+
+    def pack(index, value):
+        got = jnp.dot(ptab[index], value, preferred_element_type=f32)
+        return got.reshape(EP, K, part).astype(bf16)
+
+    def unpack(index, value):
+        flat = value.reshape(S, part)
+        return jnp.dot(whi[index, :, :S], flat, preferred_element_type=f32) + jnp.dot(
+            wlo[index, :, :S], flat, preferred_element_type=f32
+        )
+
+    for j in range(1, Z):
+        meta_copy(j).start()
+    for d in range(2):
+        @pl.when(jnp.logical_and(exists(d), jnp.logical_not(next_end(d))))
+        def _(d=d):
+            loop(0, chunks, lambda ck: own_raw(d, ck).start())
+    meta[z] = meta_ref[...]
+    for d in range(2):
+        @pl.when(jnp.logical_and(exists(d), next_end(d)))
+        def _(d=d):
+            slot = z if d == 0 else Z
+            build(z, end_of(d), Z + slot)
+
+            def chunk(ck):
+                epk[slot, :, :, cols(ck)] = pack(Z + slot, normed_ref[:, cols(ck)])
+                packed_on(d, z, slot, ck).start()
+
+            loop(0, chunks, chunk)
+    build(z, z, z)
+
+    def own_chunk(ck):
+        pk[z, :, :, cols(ck)] = pack(z, normed_ref[:, cols(ck)])
+        spread(z, ck)
+
+    loop(0, chunks, own_chunk)
+
+    def carry_on(d, src):
+        meta_arrived = pltpu.make_async_copy(meta.at[src], meta.at[src], meta_r.at[src])
+        meta_arrived.wait()
+
+        @pl.when(at_end(d))
+        def _():
+            def chunk(ck):
+                landed(pk, (src, slice(None), slice(None), cols(ck)), zr.at[src, ck])
+                spread(src, ck)
+
+            loop(0, chunks, chunk)
+
+        @pl.when(jnp.logical_not(at_end(d)))
+        def _():
+            build(src, z, src)
+
+            @pl.when(next_end(d))
+            def _():
+                build(src, end_of(d), Z + src)
+
+            def chunk(ck):
+                landed(raw, (src, slice(None), cols(ck)), zr.at[src, ck])
+
+                @pl.when(jnp.logical_not(next_end(d)))
+                def _():
+                    raw_on(d, src, ck).start()
+
+                @pl.when(next_end(d))
+                def _():
+                    epk[src, :, :, cols(ck)] = pack(Z + src, raw[src, :, cols(ck)])
+                    packed_on(d, src, src, ck).start()
+
+                pk[src, :, :, cols(ck)] = pack(src, raw[src, :, cols(ck)])
+                spread(src, ck)
+
+            loop(0, chunks, chunk)
+
+    tile = min(256, hidden)
+
+    def run_expert(src):
+        def gather(ck):
+            landed(xb, (src, slice(None), slice(None), cols(ck)), er.at[src, ck])
+            xs[:, cols(ck)] = xb[src, :, :, cols(ck)].reshape(S, part)
+
+        loop(0, chunks, gather)
+
+        def inner(n):
+            at = pl.ds(pl.multiple_of(n * tile, tile), tile)
+            gated = jnp.minimum(
+                jnp.dot(xs[...], gate_w[:, at], preferred_element_type=f32), LIMIT
+            )
+            linear = jnp.clip(
+                jnp.dot(xs[...], up_w[:, at], preferred_element_type=f32), -LIMIT, LIMIT
+            )
+            act[:, at] = (gated * jax.nn.sigmoid(SLOPE * gated) * (linear + 1.0)).astype(bf16)
+
+        loop(0, hidden // tile, inner)
+
+        def outer(ck):
+            result = jnp.dot(act[...], down_w[:, cols(ck)], preferred_element_type=f32)
+            xb[src, :, :, cols(ck)] = result.reshape(EP, K, part).astype(bf16)
+            give_back(src, ck)
+
+        loop(0, chunks, outer)
+
+    def far_slot(d, src):
+        return src if d == 0 else jnp.where(z + 1 == src, Z, src)
+
+    def back_packed(d, src, ck):
+        return remote(
+            rb.at[src, :, :, cols(ck)], fp.at[far_slot(d, src), :, :, cols(ck)],
+            fs.at[src, ck], fa.at[far_slot(d, src), ck], side(1 - d),
+        )
+
+    def back_raw(d, src, ck):
+        return remote(
+            raw.at[src, :, cols(ck)], fr.at[far_slot(d, src), :, cols(ck)],
+            fs.at[src, ck], fa.at[far_slot(d, src), ck], side(1 - d),
+        )
+
+    def add_far(d, slot, ck):
+        @pl.when(next_end(d))
+        def _():
+            landed(fp, (slot, slice(None), slice(None), cols(ck)), fa.at[slot, ck])
+            acc[...] += unpack(Z + slot, fp[slot, :, :, cols(ck)])
+
+        @pl.when(jnp.logical_not(next_end(d)))
+        def _():
+            landed(fr, (slot, slice(None), cols(ck)), fa.at[slot, ck])
+            acc[...] += fr[slot, :, cols(ck)].astype(f32)
+
+    def returned(src, ck):
+        landed(rb, (src, slice(None), slice(None), cols(ck)), rr.at[src, ck])
+
+    def send_back(d, src):
+        def chunk(ck):
+            returned(src, ck)
+
+            @pl.when(at_end(d))
+            def _():
+                back_packed(d, src, ck).start()
+
+            @pl.when(jnp.logical_not(at_end(d)))
+            def _():
+                acc[...] = unpack(src, rb[src, :, :, cols(ck)])
+                add_far(d, src, ck)
+
+                @pl.when(jnp.logical_not(next_end(d)))
+                def _():
+                    raw_on(d, src, ck).wait_send()
+
+                raw[src, :, cols(ck)] = acc[...].astype(bf16)
+                back_raw(d, src, ck).start()
+
+        loop(0, chunks, chunk)
+
+    def wait_weights():
+        for copy in weights:
+            copy.wait()
+
+    def stage(s):
+        for d in range(2):
+            src = z - s if d == 0 else z + s
+
+            @pl.when(src >= 0 if d == 0 else src < Z)
+            def _(d=d, src=src):
+                carry_on(d, src)
+
+        @pl.when(s == 1)
+        def _():
+            wait_weights()
+
+        def expert(t):
+            src = jnp.where(t == 0, z, jnp.where(t == 1, z - s, z + s))
+            fits = jnp.logical_and(src >= 0, src < Z)
+
+            @pl.when(jnp.logical_and(fits, jnp.logical_or(t > 0, s == 1)))
+            def _():
+                run_expert(src)
+
+        loop(0, 3, expert)
+        for d in range(2):
+            src = Z - 1 - s if d == 0 else s + 0 * z
+
+            @pl.when(src < z if d == 0 else src > z)
+            def _(d=d, src=src):
+                send_back(d, src)
+
+    if Z > 1:
+        loop(1, Z, stage)
+    else:
+        wait_weights()
+        run_expert(z)
+
+    def finish(ck):
+        returned(z, ck)
+        acc[...] = upd_ref[:, cols(ck)].astype(f32) + unpack(z, rb[z, :, :, cols(ck)])
+        for d in range(2):
+            @pl.when(exists(d))
+            def _(d=d):
+                add_far(d, z if d == 0 else Z, ck)
+        out_ref[:, cols(ck)] = acc[...].astype(bf16)
+
+    loop(0, chunks, finish)
+
+    for j in range(1, Z):
+        meta_copy(j).wait_send()
+
+    def sent_all(ck):
+        for d in range(2):
+            @pl.when(jnp.logical_and(exists(d), jnp.logical_not(next_end(d))))
+            def _(d=d):
+                own_raw(d, ck).wait_send()
+
+            @pl.when(jnp.logical_and(exists(d), next_end(d)))
+            def _(d=d):
+                packed_on(d, z, z if d == 0 else Z, ck).wait_send()
+
+        def per_source(src):
+            some = pl.ds(0, EP - 1)
+            landed(pk, (src, some, slice(None), cols(ck)), es.at[src, ck])
+            landed(xb, (src, some, slice(None), cols(ck)), rs.at[src, ck])
+            for d in range(2):
+                @pl.when(src < z if d == 0 else src > z)
+                def _(d=d):
+                    @pl.when(at_end(d))
+                    def _():
+                        back_packed(d, src, ck).wait_send()
+
+                    @pl.when(jnp.logical_not(at_end(d)))
+                    def _():
+                        back_raw(d, src, ck).wait_send()
+
+                        @pl.when(next_end(d))
+                        def _():
+                            packed_on(d, src, src, ck).wait_send()
+
+        loop(0, Z, per_source)
+
+    loop(0, chunks, sent_all)
+
+
+def experts(route_ids, route_weight, normed, updated, gate_matrix, up_matrix, down_matrix):
+    sp_count, dp_count = lax.axis_size("sp"), lax.axis_size("dp")
+    planes = 4 if sp_count % 4 == 0 else 1
+    lanes_x = sp_count // planes
+    rows, width = normed.shape
+    top = route_ids.shape[1]
+    capacity = max(2, 3 * rows * top // (2 * sp_count * dp_count))
+    slots = -(-capacity // 8) * 8
+    group = lanes_x * dp_count
+    padded = -(-group * slots // 128) * 128
+    hidden = gate_matrix.shape[1]
+    chunks = CHUNKS if width % (128 * CHUNKS) == 0 else 1
+    meta = jnp.concatenate([route_ids.astype(jnp.float32), route_weight], axis=1).T
+    dma = pltpu.SemaphoreType.DMA
+    vmem = pl.BlockSpec(memory_space=pltpu.VMEM)
+    hbm = pl.BlockSpec(memory_space=pl.ANY)
+    bf16, f32 = jnp.bfloat16, jnp.float32
+    return pl.pallas_call(
+        functools.partial(experts_kernel, planes, lanes_x, slots),
+        name="routed_experts",
+        out_shape=jax.ShapeDtypeStruct((rows, width), bf16),
+        in_specs=[vmem] * 3 + [hbm] * 3,
+        out_specs=vmem,
+        scratch_shapes=[
+            pltpu.VMEM((planes, 2 * top, rows), f32),
+            pltpu.VMEM((planes, rows, width), bf16),
+            pltpu.VMEM((planes, group, slots, width), bf16),
+            pltpu.VMEM((planes + 1, group, slots, width), bf16),
+            pltpu.VMEM((planes, group, slots, width), bf16),
+            pltpu.VMEM((planes, group, slots, width), bf16),
+            pltpu.VMEM((planes + 1, rows, width), bf16),
+            pltpu.VMEM((planes + 1, group, slots, width), bf16),
+            pltpu.VMEM((2 * planes + 1, group * slots, rows), bf16),
+            pltpu.VMEM((2 * planes + 1, rows, padded), bf16),
+            pltpu.VMEM((2 * planes + 1, rows, padded), bf16),
+            pltpu.VMEM((rows, rows), bf16),
+            pltpu.VMEM((group * slots, width), bf16),
+            pltpu.VMEM((group * slots, hidden), bf16),
+            pltpu.VMEM((rows, width // chunks), f32),
+            pltpu.VMEM(gate_matrix.shape, bf16),
+            pltpu.VMEM(up_matrix.shape, bf16),
+            pltpu.VMEM(down_matrix.shape, bf16),
+            dma((planes,)), dma((planes,)),
+            dma((planes + 1, chunks)), dma((planes, chunks)),
+            dma((planes, chunks)), dma((planes, chunks)),
+            dma((planes, chunks)), dma((planes, chunks)),
+            dma((planes, chunks)), dma((planes + 1, chunks)),
+            dma((3,)),
+        ],
+        compiler_params=pltpu.CompilerParams(
+            collective_id=1, has_side_effects=True, vmem_limit_bytes=VMEM_BYTES
+        ),
+    )(meta, normed, updated, gate_matrix, up_matrix, down_matrix)
 
 
 def per_device(
@@ -397,43 +838,17 @@
     expert_up,
     expert_down,
 ):
-    span_devices = lax.axis_size("sp")
-    experts_total = span_devices * lax.axis_size("dp")
     tok_rows = resid.shape[1]
-    model_width = resid.shape[2]
     head_dim = q_gain.shape[0]
     places = lax.axis_index("sp") * tok_rows + jnp.arange(tok_rows, dtype=jnp.int32)
     cosine, sine = turn_tables(places, head_dim)
     updated, normed = attention(
         query[0], keys[0], values[0], q_gain, k_gain, cosine, sine, resid[0], norm_gain, out_weight
     )
-    widened = updated.astype(jnp.float32)
-    top_count = route_ids.shape[2]
-    capacity = max(2, 3 * tok_rows * top_count // (2 * experts_total))
-    chosen = route_ids[0].reshape(-1)
-    onehot = (chosen[:, None] == jnp.arange(experts_total, dtype=jnp.int32)[None, :]).astype(
-        jnp.int32
-    )
-    earlier = jnp.sum((jnp.cumsum(onehot, axis=0) - onehot) * onehot, axis=1)
-    target = chosen * capacity + earlier
-    sources = jnp.arange(tok_rows * top_count, dtype=jnp.int32) // top_count
-    slot_table = jnp.full((experts_total * capacity,), tok_rows, jnp.int32).at[target].set(sources)
-    padded = jnp.concatenate([normed, jnp.zeros((1, model_width), jnp.bfloat16)], axis=0)
-    outgoing = padded[slot_table].reshape(experts_total, capacity, model_width)
-    answered = apply_expert(
-        lax.all_to_all(outgoing, ("sp", "dp"), split_axis=0, concat_axis=0, tiled=True),
-        expert_gate[0],
-        expert_up[0],
-        expert_down[0],
-    )
-    returned = lax.all_to_all(answered, ("sp", "dp"), split_axis=0, concat_axis=0, tiled=True)
-    rows_back = returned.reshape(experts_total * capacity, model_width)
-    slots = target.reshape(tok_rows, top_count)
-    combined = sum(
-        rows_back[slots[:, i]].astype(jnp.float32) * route_weight[0, :, i][:, None]
-        for i in range(top_count)
-    )
-    return (widened + combined).astype(jnp.bfloat16)[None]
+    return experts(
+        route_ids[0], route_weight[0], normed, updated,
+        expert_gate[0], expert_up[0], expert_down[0],
+    )[None]
 
 
 def solution(mesh):

time: 265 us -> 243 us (0.917)
  the two profiles are of different devices: /device:TPU:0 before, /device:TPU:28 now
where the time goes in v1:
time: 243 us
  Pallas kernels  236 us (97%)
  other arithmetic  4.64 us (2%)
    pallas_call x1, Pallas kernels, experts(): pl.pallas_call(functools.partial(experts_kernel, planes, lanes_x, slots),...  159 us
    pallas_call x1, Pallas kernels, attention(): pl.pallas_call(functools.partial(attention_kernel, planes, lanes_x, outer...  77 us

profile of v1, /device:TPU:28, one launch (start us, length us, event | category | flops | bytes accessed | tf_op | source)
XLA Modules:
  0.0 243.0 jit_solution(18204608956705186571)
XLA Ops:
  0.0 0.7 convert_bitcast_fusion
  0.7 1.3 maximum_bitcast_fusion.meta_ref
  2.0 1.0 fusion
  3.0 0.8 pad_maximum_fusion.1.sin_ref
  3.8 0.8 pad_maximum_fusion.cos_ref
  4.7 77.0 %gathered_attention.1 = (bf16[256,2048]{1,0:T(8,128)(2,1)}, bf16[256,2048]{1,0:T(8,128)(2,1)}) custom-call(bf16[256,2048]{1,0:T(8,128)(2,1)} %bitcast.20, bf16[256,512]{1,0:T(8,128)(2,1)} %bitcast.22, bf16[256,512]{1,0:T(8,128)(2,1)} %bitcast.23, f32[1,128]{1,0:T(1,128)} %bitcast.26, f32[1,128]{1,0:T(1,128)} %bitcast.27, ...), custom_call_target="tpu_custom_call" | custom-call | tf_op jit(solution)/shard_map/gathered_attention/pallas_call | solution.py:335
  81.7 159.0 %routed_experts.1 = bf16[256,2048]{1,0:T(8,128)(2,1)} custom-call(f32[4,256]{1,0:T(4,128)} %maximum_bitcast_fusion.meta_ref, bf16[256,2048]{1,0:T(8,128)(2,1)} %get-tuple-element.7.normed_ref, bf16[256,2048]{1,0:T(8,128)(2,1)} %get-tuple-element.8.upd_ref, bf16[2048,1024]{1,0:T(8,128)(2,1)} %bitcast.16, bf16[2048,1024]{1,0:T(8,128)(2,1)} %bitcast.17, ...), custom_call_target="tpu_custom_call" | custom-call | tf_op jit(solution)/shard_map/routed_experts/pallas_call | solution.py:788
  240.7 2.3 copy.17
  (2 shorter events, 0.0 us)

commit v2 on v1

--- a/solution.py
+++ b/solution.py
@@ -430,20 +430,26 @@
     ).astype(f32).astype(bf16)
     pl.semaphore_wait(barrier, EP - 1 + Z - 1)
 
+    def toward(d):
+        return 1 - 2 * d
+
     def side(d):
-        return (sp + X if d == 0 else sp - X, dp)
+        return (sp + X * toward(d), dp)
+
+    def end_of(d):
+        return (Z - 1) * (1 - d)
 
     def exists(d):
-        return z + 1 < Z if d == 0 else z >= 1
+        return jnp.logical_and(z + toward(d) >= 0, z + toward(d) < Z)
 
     def at_end(d):
-        return z == Z - 1 if d == 0 else z == 0
+        return z == end_of(d)
 
     def next_end(d):
-        return z + 1 == Z - 1 if d == 0 else z - 1 == 0
-
-    def end_of(d):
-        return Z - 1 if d == 0 else 0
+        return z + toward(d) == end_of(d)
+
+    def own_slot(d):
+        return z + d * (Z - z)
 
     def meta_copy(j):
         return remote(
@@ -453,7 +459,7 @@
     def own_raw(d, ck):
         return remote(
             normed_ref.at[:, cols(ck)], raw.at[z, :, cols(ck)],
-            zs.at[z if d == 0 else Z, ck], zr.at[z, ck], side(d),
+            zs.at[own_slot(d), ck], zr.at[z, ck], side(d),
         )
 
     def raw_on(d, src, ck):
@@ -502,11 +508,9 @@
 
     def build(src, plane, index):
         info = meta[src]
-        lane_expert = lax.broadcasted_iota(jnp.int32, (EP, rows), 0).astype(f32) + (
-            plane * EP
-        ).astype(f32) if not isinstance(plane, int) else (
-            lax.broadcasted_iota(jnp.int32, (EP, rows), 0).astype(f32) + float(plane * EP)
-        )
+        lane_expert = (
+            lax.broadcasted_iota(jnp.int32, (EP, rows), 0) + plane * EP
+        ).astype(f32)
         named = jnp.zeros((EP, rows), f32)
         scale = jnp.zeros((EP, rows), f32)
         for i in range(top):
@@ -542,22 +546,37 @@
 
     for j in range(1, Z):
         meta_copy(j).start()
-    for d in range(2):
+
+    def own_raw_start(d):
         @pl.when(jnp.logical_and(exists(d), jnp.logical_not(next_end(d))))
-        def _(d=d):
+        def _():
             loop(0, chunks, lambda ck: own_raw(d, ck).start())
+
+    loop(0, 2, own_raw_start)
     meta[z] = meta_ref[...]
-    for d in range(2):
+
+    def own_packed(d, low, high):
         @pl.when(jnp.logical_and(exists(d), next_end(d)))
-        def _(d=d):
-            slot = z if d == 0 else Z
-            build(z, end_of(d), Z + slot)
+        def _():
+            slot = own_slot(d)
 
             def chunk(ck):
                 epk[slot, :, :, cols(ck)] = pack(Z + slot, normed_ref[:, cols(ck)])
                 packed_on(d, z, slot, ck).start()
 
-            loop(0, chunks, chunk)
+            loop(low, high, chunk)
+
+    def own_packed_start(d):
+        @pl.when(jnp.logical_and(exists(d), next_end(d)))
+        def _():
+            build(z, end_of(d), Z + own_slot(d))
+
+        own_packed(d, 0, early)
+
+    early = -(-chunks // 2)
+    last = chunks - 1
+    is_end = jnp.logical_or(z == 0, z == Z - 1)
+    loop(0, 2, own_packed_start)
     build(z, z, z)
 
     def own_chunk(ck):
@@ -566,46 +585,43 @@
 
     loop(0, chunks, own_chunk)
 
-    def carry_on(d, src):
-        meta_arrived = pltpu.make_async_copy(meta.at[src], meta.at[src], meta_r.at[src])
-        meta_arrived.wait()
+    def carry_on(d, src, ck):
+        @pl.when(ck == 0)
+        def _():
+            pltpu.make_async_copy(meta.at[src], meta.at[src], meta_r.at[src]).wait()
 
         @pl.when(at_end(d))
         def _():
-            def chunk(ck):
-                landed(pk, (src, slice(None), slice(None), cols(ck)), zr.at[src, ck])
-                spread(src, ck)
-
-            loop(0, chunks, chunk)
+            landed(pk, (src, slice(None), slice(None), cols(ck)), zr.at[src, ck])
+            spread(src, ck)
 
         @pl.when(jnp.logical_not(at_end(d)))
         def _():
-            build(src, z, src)
-
-            @pl.when(next_end(d))
-            def _():
-                build(src, end_of(d), Z + src)
-
-            def chunk(ck):
-                landed(raw, (src, slice(None), cols(ck)), zr.at[src, ck])
-
-                @pl.when(jnp.logical_not(next_end(d)))
-                def _():
-                    raw_on(d, src, ck).start()
+            @pl.when(ck == 0)
+            def _():
+                build(src, z, src)
 
                 @pl.when(next_end(d))
                 def _():
-                    epk[src, :, :, cols(ck)] = pack(Z + src, raw[src, :, cols(ck)])
-                    packed_on(d, src, src, ck).start()
-
-                pk[src, :, :, cols(ck)] = pack(src, raw[src, :, cols(ck)])
-                spread(src, ck)
-
-            loop(0, chunks, chunk)
+                    build(src, end_of(d), Z + src)
+
+            landed(raw, (src, slice(None), cols(ck)), zr.at[src, ck])
+
+            @pl.when(jnp.logical_not(next_end(d)))
+            def _():
+                raw_on(d, src, ck).start()
+
+            @pl.when(next_end(d))
+            def _():
+                epk[src, :, :, cols(ck)] = pack(Z + src, raw[src, :, cols(ck)])
+                packed_on(d, src, src, ck).start()
+
+            pk[src, :, :, cols(ck)] = pack(src, raw[src, :, cols(ck)])
+            spread(src, ck)
 
     tile = min(256, hidden)
 
-    def run_expert(src):
+    def run_expert(src, now):
         def gather(ck):
             landed(xb, (src, slice(None), slice(None), cols(ck)), er.at[src, ck])
             xs[:, cols(ck)] = xb[src, :, :, cols(ck)].reshape(S, part)
@@ -627,12 +643,14 @@
         def outer(ck):
             result = jnp.dot(act[...], down_w[:, cols(ck)], preferred_element_type=f32)
             xb[src, :, :, cols(ck)] = result.reshape(EP, K, part).astype(bf16)
-            give_back(src, ck)
+
+            if now:
+                give_back(src, ck)
 
         loop(0, chunks, outer)
 
     def far_slot(d, src):
-        return src if d == 0 else jnp.where(z + 1 == src, Z, src)
+        return jnp.where(jnp.logical_and(d == 1, z + 1 == src), Z, src)
 
     def back_packed(d, src, ck):
         return remote(
@@ -660,73 +678,131 @@
     def returned(src, ck):
         landed(rb, (src, slice(None), slice(None), cols(ck)), rr.at[src, ck])
 
-    def send_back(d, src):
-        def chunk(ck):
-            returned(src, ck)
-
-            @pl.when(at_end(d))
-            def _():
-                back_packed(d, src, ck).start()
-
-            @pl.when(jnp.logical_not(at_end(d)))
-            def _():
-                acc[...] = unpack(src, rb[src, :, :, cols(ck)])
-                add_far(d, src, ck)
-
-                @pl.when(jnp.logical_not(next_end(d)))
-                def _():
-                    raw_on(d, src, ck).wait_send()
-
-                raw[src, :, cols(ck)] = acc[...].astype(bf16)
-                back_raw(d, src, ck).start()
-
-        loop(0, chunks, chunk)
+    def send_back(d, src, ck):
+        returned(src, ck)
+
+        @pl.when(at_end(d))
+        def _():
+            back_packed(d, src, ck).start()
+
+        @pl.when(jnp.logical_not(at_end(d)))
+        def _():
+            acc[...] = unpack(src, rb[src, :, :, cols(ck)])
+            add_far(d, src, ck)
+
+            @pl.when(jnp.logical_not(next_end(d)))
+            def _():
+                raw_on(d, src, ck).wait_send()
+
+            raw[src, :, cols(ck)] = acc[...].astype(bf16)
+            back_raw(d, src, ck).start()
 
     def wait_weights():
         for copy in weights:
             copy.wait()
 
+    def backward(k):
+        def chunk(ck):
+            def one(t):
+                d = jnp.where(2 * z >= Z, t, 1 - t)
+                src = (Z - 1 - k) * (1 - d) + k * d
+
+                @pl.when((z - src) * toward(d) > 0)
+                def _():
+                    send_back(d, src, ck)
+
+            loop(0, 2, one)
+
+        loop(0, chunks, chunk)
+
+    def away(s):
+        if Z < 3:
+            return s
+        return jnp.where(jnp.logical_and(is_end, jnp.logical_and(s > 0, s < 3)), 3 - s, s)
+
+    def inward(t):
+        return jnp.where(2 * z >= Z, t, 1 - t)
+
+    def within(src):
+        return jnp.logical_and(src >= 0, src < Z)
+
     def stage(s):
-        for d in range(2):
-            src = z - s if d == 0 else z + s
-
-            @pl.when(src >= 0 if d == 0 else src < Z)
-            def _(d=d, src=src):
-                carry_on(d, src)
-
-        @pl.when(s == 1)
-        def _():
-            wait_weights()
-
-        def expert(t):
-            src = jnp.where(t == 0, z, jnp.where(t == 1, z - s, z + s))
-            fits = jnp.logical_and(src >= 0, src < Z)
-
-            @pl.when(jnp.logical_and(fits, jnp.logical_or(t > 0, s == 1)))
-            def _():
-                run_expert(src)
-
-        loop(0, 3, expert)
-        for d in range(2):
-            src = Z - 1 - s if d == 0 else s + 0 * z
-
-            @pl.when(src < z if d == 0 else src > z)
-            def _(d=d, src=src):
-                send_back(d, src)
-
+        def chunk(ck):
+            def one(d):
+                src = z - away(s) * toward(d)
+
+                @pl.when(within(src))
+                def _():
+                    carry_on(d, src, ck)
+
+            loop(0, 2, one)
+
+            @pl.when(jnp.logical_and(s == 1, ck == 0))
+            def _():
+                wait_weights()
+
+            def expert(far, t, now):
+                src = z - far * toward(inward(t))
+
+                @pl.when(within(src))
+                def _():
+                    run_expert(src, now)
+
+            middle = jnp.logical_and(s > 1, jnp.logical_not(is_end))
+            late_end = jnp.logical_and(is_end, s == 3)
+            first = jnp.where(is_end, min(1, last), 0)
+
+            @pl.when(jnp.logical_and(jnp.logical_and(s > 1, ck == first), jnp.logical_not(late_end)))
+            def _():
+                expert(away(s - 1), 0, True)
+
+            @pl.when(jnp.logical_and(middle, ck == min(1, last)))
+            def _():
+                expert(s - 1, 1, False)
+
+            @pl.when(ck == last)
+            def _():
+                @pl.when(s == 1)
+                def _():
+                    loop(0, 2, lambda d: own_packed(d, early, chunks))
+                    run_expert(z, False)
+
+                src = z - (s - 1) * toward(inward(1))
+
+                @pl.when(jnp.logical_and(middle, within(src)))
+                def _():
+                    loop(0, chunks, lambda i: give_back(src, i))
+
+                @pl.when(s == Z)
+                def _():
+                    if Z > 2:
+                        @pl.when(is_end)
+                        def _():
+                            expert(away(2), 0, True)
+                    loop(0, chunks, lambda i: give_back(z, i))
+
+            turn = jnp.where(jnp.logical_and(is_end, s < Z), 0, last)
+
+            @pl.when(jnp.logical_and(s > 2, ck == turn))
+            def _():
+                backward(s - 1)
+
+        loop(0, chunks, chunk)
+
+    loop(1, Z + 1, stage)
     if Z > 1:
-        loop(1, Z, stage)
-    else:
-        wait_weights()
-        run_expert(z)
+        backward(1)
 
     def finish(ck):
         returned(z, ck)
         acc[...] = upd_ref[:, cols(ck)].astype(f32) + unpack(z, rb[z, :, :, cols(ck)])
-        for d in range(2):
+
+        def beyond(d):
             @pl.when(exists(d))
-            def _(d=d):
-                add_far(d, z if d == 0 else Z, ck)
+            def _():
+                add_far(d, own_slot(d), ck)
+
+        loop(0, 2, beyond)
         out_ref[:, cols(ck)] = acc[...].astype(bf16)
 
     loop(0, chunks, finish)
@@ -735,33 +811,36 @@
         meta_copy(j).wait_send()
 
     def sent_all(ck):
-        for d in range(2):
+        def own_sent(d):
             @pl.when(jnp.logical_and(exists(d), jnp.logical_not(next_end(d))))
-            def _(d=d):
+            def _():
                 own_raw(d, ck).wait_send()
 
             @pl.when(jnp.logical_and(exists(d), next_end(d)))
-            def _(d=d):
-                packed_on(d, z, z if d == 0 else Z, ck).wait_send()
+            def _():
+                packed_on(d, z, own_slot(d), ck).wait_send()
+
+        loop(0, 2, own_sent)
 
         def per_source(src):
             some = pl.ds(0, EP - 1)
             landed(pk, (src, some, slice(None), cols(ck)), es.at[src, ck])
             landed(xb, (src, some, slice(None), cols(ck)), rs.at[src, ck])
-            for d in range(2):
-                @pl.when(src < z if d == 0 else src > z)
-                def _(d=d):
-                    @pl.when(at_end(d))
+            d = jnp.where(src < z, 0, 1)
+
+            @pl.when(src != z)
+            def _():
+                @pl.when(at_end(d))
+                def _():
+                    back_packed(d, src, ck).wait_send()
+
+                @pl.when(jnp.logical_not(at_end(d)))
+                def _():
+                    back_raw(d, src, ck).wait_send()
+
+                    @pl.when(next_end(d))
                     def _():
-                        back_packed(d, src, ck).wait_send()
-
-                    @pl.when(jnp.logical_not(at_end(d)))
-                    def _():
-                        back_raw(d, src, ck).wait_send()
-
-                        @pl.when(next_end(d))
-                        def _():
-                            packed_on(d, src, src, ck).wait_send()
+                        packed_on(d, src, src, ck).wait_send()
 
         loop(0, Z, per_source)
 

time: 243 us -> 209 us (0.86)
  the two profiles are of different devices: /device:TPU:28 before, /device:TPU:0 now
where the time goes in v2:
time: 209 us
  Pallas kernels  202 us (97%)
  other arithmetic  4.64 us (2%)
  local copies, waits for them, and re-layouts  2.3 us (1%)
    pallas_call x1, Pallas kernels, experts(): pl.pallas_call(functools.partial(experts_kernel, planes, lanes_x, slots),...  123 us
    pallas_call x1, Pallas kernels, attention(): pl.pallas_call(functools.partial(attention_kernel, planes, lanes_x, outer...  79.6 us

profile of v2, /device:TPU:0, one launch (start us, length us, event | category | flops | bytes accessed | tf_op | source)
XLA Modules:
  0.0 209.1 jit_solution(9963871181274499252)
XLA Ops:
  0.0 0.7 convert_bitcast_fusion
  0.7 1.3 maximum_bitcast_fusion.meta_ref
  2.0 1.0 fusion
  3.0 0.8 pad_maximum_fusion.1.sin_ref
  3.8 0.8 pad_maximum_fusion.cos_ref
  4.7 79.6 %gathered_attention.1 = (bf16[256,2048]{1,0:T(8,128)(2,1)}, bf16[256,2048]{1,0:T(8,128)(2,1)}) custom-call(bf16[256,2048]{1,0:T(8,128)(2,1)} %bitcast.20, bf16[256,512]{1,0:T(8,128)(2,1)} %bitcast.22, bf16[256,512]{1,0:T(8,128)(2,1)} %bitcast.23, f32[1,128]{1,0:T(1,128)} %bitcast.26, f32[1,128]{1,0:T(1,128)} %bitcast.27, ...), custom_call_target="tpu_custom_call" | custom-call | tf_op jit(solution)/shard_map/gathered_attention/pallas_call | solution.py:335
  84.3 122.5 %routed_experts.1 = bf16[256,2048]{1,0:T(8,128)(2,1)} custom-call(f32[4,256]{1,0:T(4,128)} %maximum_bitcast_fusion.meta_ref, bf16[256,2048]{1,0:T(8,128)(2,1)} %get-tuple-element.7.normed_ref, bf16[256,2048]{1,0:T(8,128)(2,1)} %get-tuple-element.8.upd_ref, bf16[2048,1024]{1,0:T(8,128)(2,1)} %bitcast.16, bf16[2048,1024]{1,0:T(8,128)(2,1)} %bitcast.17, ...), custom_call_target="tpu_custom_call" | custom-call | tf_op jit(solution)/shard_map/routed_experts/pallas_call | solution.py:867
  206.8 2.3 %copy.17 = bf16[1,256,2048]{2,1,0:T(8,128)(2,1)} copy(bf16[1,256,2048]{2,1,0:T(8,128)(2,1)} %bitcast.19) | data formatting | bytes 2097152
  (2 shorter events, 0.0 us)

commit v3 on v2

--- a/solution.py
+++ b/solution.py
@@ -39,7 +39,8 @@
     q_ref, k_ref, v_ref, qg_ref, kg_ref, cos_ref, sin_ref, resid_ref, ng_ref, w_ref,
     upd_ref, normed_ref,
     kall, vall, wall, qt, acc, mx, ls, head_out,
-    kx_s, kx_r, kz_s, kz_r, vz_s, vz_r, vx_s, vx_r, wy_s, wy_r, wc_s, wc_r, loc,
+    kx_s, kx_r, kz_s, kz_r, hz_s, hz_r, hx_s, hx_r, vz_s, vz_r, vx_s, vx_r,
+    wy_s, wy_r, wc_s, wc_r, loc,
 ):
     Z, X, Y, C = planes, lanes_x, outer_dp, inner_dp
     rows, head_dim = cos_ref.shape
@@ -112,42 +113,83 @@
             device_id=device, device_id_type=MESH,
         )
 
+    split = kv_heads // 2 * head_dim
+    low, high = slice(0, split), slice(split, kv_heads * head_dim)
+
+    def toward(d):
+        return 1 - 2 * d
+
+    def across(j):
+        return (z * X + (x + j) % X, dp)
+
+    def onward(d):
+        return (sp + X * toward(d), dp)
+
+    def source(d, s):
+        return z - s * toward(d)
+
+    def hop(d, s):
+        return d * (Z - 1) + s
+
+    def loop(first_index, last_index, body):
+        def step(i, carry):
+            body(i)
+            return carry
+        lax.fori_loop(first_index, last_index, step, 0)
+
     def kx(j):
-        return remote(kall, krows(sp), kx_s.at[j], kx_r.at[j], (z * X + (x + j) % X, dp))
+        return remote(kall, (krows(sp), low), kx_s.at[j], kx_r.at[j], across(j))
 
     def kz(d, s, j):
-        plane = z - s if d == 0 else z + s
-        device = (sp + X if d == 0 else sp - X, dp)
-        at = (d * (Z - 1) + s) * X + j
-        return remote(kall, krows(plane * X + (x + X - j) % X), kz_s.at[at], kz_r.at[at], device)
+        at = hop(d, s) * X + j
+        block = source(d, s) * X + (x + X - j) % X
+        return remote(kall, (krows(block), low), kz_s.at[at], kz_r.at[at], onward(d))
+
+    def hz(d, s):
+        at = hop(d, s)
+        return remote(
+            kall, (krows(source(d, s) * X + x), high), hz_s.at[at], hz_r.at[at], onward(d)
+        )
 
     def vz(d, s):
-        plane = z - s if d == 0 else z + s
-        device = (sp + X if d == 0 else sp - X, dp)
-        at = d * (Z - 1) + s
-        return remote(vall, krows(plane * X + x), vz_s.at[at], vz_r.at[at], device)
+        at = hop(d, s)
+        return remote(vall, (krows(source(d, s) * X + x),), vz_s.at[at], vz_r.at[at], onward(d))
+
+    def hx(slot, plane, j):
+        at = slot * X + j
+        return remote(
+            kall, (krows(plane * X + x), high), hx_s.at[at], hx_r.at[at], across(j)
+        )
 
     def vx(slot, plane, j):
         at = slot * X + j
+        return remote(vall, (krows(plane * X + x),), vx_s.at[at], vx_r.at[at], across(j))
+
+    def valid(plane):
+        return jnp.logical_and(plane >= 0, plane < Z)
+
+    def sends(d, s):
+        return jnp.logical_and(valid(z + toward(d)), valid(source(d, s)))
+
+    def gets(d, s):
+        return valid(source(d, s + 1))
+
+    pieces = wy_s.shape[0] // Y
+    w_part = w_rows // pieces
+
+    def wpart(block, h):
+        return pl.ds(pl.multiple_of(block * w_rows + h * w_part, w_part), w_part)
+
+    def wy(j, h):
+        at = j * pieces + h
         return remote(
-            vall, krows(plane * X + x), vx_s.at[at], vx_r.at[at], (z * X + (x + j) % X, dp)
-        )
-
-    def sends(d, s):
-        if d == 0:
-            return jnp.logical_and(up_ok, z - s >= 0)
-        return jnp.logical_and(down_ok, z + s < Z)
-
-    def gets(d, s):
-        return z - s - 1 >= 0 if d == 0 else z + s + 1 < Z
-
-    def wy(j):
-        return remote(wall, wrows(dp), wy_s.at[j], wy_r.at[j], (sp, ((y + j) % Y) * C + c))
-
-    def wc(j, i):
-        at = j * C + i
+            wall, (wpart(dp, h),), wy_s.at[at], wy_r.at[at], (sp, ((y + j) % Y) * C + c)
+        )
+
+    def wc(j, i, h):
+        at = (j * C + i) * pieces + h
         return remote(
-            wall, wrows(((y + Y - j) % Y) * C + c), wc_s.at[at], wc_r.at[at],
+            wall, (wpart(((y + Y - j) % Y) * C + c, h),), wc_s.at[at], wc_r.at[at],
             (sp, y * C + (c + i) % C),
         )
 
@@ -156,14 +198,17 @@
     for d in range(2):
         @pl.when(sends(d, 0))
         def _(d=d):
+            vz(d, 0).start()
+            hz(d, 0).start()
             kz(d, 0, 0).start()
-            vz(d, 0).start()
     for j in range(1, X):
+        hx(0, z, j).start()
         vx(0, z, j).start()
-    for j in range(1, Y):
-        wy(j).start()
-    for i in range(1, C):
-        wc(0, i).start()
+    for h in range(pieces):
+        for j in range(1, Y):
+            wy(j, h).start()
+        for i in range(1, C):
+            wc(0, i, h).start()
 
     def prepare_queries(h, carry):
         at = pl.ds(pl.multiple_of(h * head_dim, head_dim), head_dim)
@@ -217,62 +262,104 @@
 
         lax.fori_loop(0, kv_heads, one_group, 0)
 
-    def wait_vx(slot, plane):
+    def wait_across(slot, plane):
         for j in range(1, X):
+            hx(slot, plane, j).wait_recv()
             vx(slot, plane, j).wait_recv()
 
-    def attend_step(s):
-        def one(t, carry):
-            plane = jnp.where(t == 0, z - s - 1, z + s + 1)
-
-            @pl.when(jnp.logical_and(plane >= 0, plane < Z))
-            def _():
-                wait_vx(1 + s + t * (Z - 1), plane)
-                attend(plane, False)
-            return carry
-
-        lax.fori_loop(0, 2, one, 0)
-
-    for s in range(Z - 1):
-        for d in range(2):
+    def inward(t):
+        return jnp.where(2 * z >= Z, t, 1 - t)
+
+    def open_step(s):
+        def one(t):
+            d = inward(t)
+
             @pl.when(gets(d, s))
-            def _(d=d, s=s):
-                plane = z - s - 1 if d == 0 else z + s + 1
+            def _():
+                plane, slot = source(d, s + 1), 1 + hop(d, s)
+                more = jnp.logical_and(s + 1 < Z - 1, sends(d, s + 1))
                 vz(d, s).wait_recv()
                 for j in range(1, X):
-                    vx(1 + s + d * (Z - 1), plane, j).start()
-                if s + 1 < Z - 1:
-                    @pl.when(sends(d, s + 1))
-                    def _():
-                        vz(d, s + 1).start()
+                    vx(slot, plane, j).start()
+
+                @pl.when(more)
+                def _():
+                    vz(d, s + 1).start()
+
+                hz(d, s).wait_recv()
+                for j in range(1, X):
+                    hx(slot, plane, j).start()
+
+                @pl.when(more)
+                def _():
+                    hz(d, s + 1).start()
+
+        loop(0, 2, one)
+
+    def close_step(s):
+        def one(t):
+            d = inward(t)
+
+            @pl.when(gets(d, s))
+            def _():
+                more = jnp.logical_and(s + 1 < Z - 1, sends(d, s + 1))
                 for j in range(X):
                     kz(d, s, j).wait_recv()
-                    if s + 1 < Z - 1:
-                        @pl.when(sends(d, s + 1))
-                        def _(j=j):
-                            kz(d, s + 1, j).start()
-        if s == 0:
-            wait_vx(0, z)
-            attend(z, True)
-        else:
-            attend_step(s - 1)
-
-    for j in range(1, Y):
-        wy(j).wait_recv()
-        for i in range(1, C):
-            wc(j, i).start()
-    if Z == 1:
-        wait_vx(0, z)
-        attend(z, True)
+
+                    @pl.when(more)
+                    def _(j=j):
+                        kz(d, s + 1, j).start()
+
+        loop(0, 2, one)
+
+    def pass_weights():
+        for h in range(pieces):
+            for j in range(1, Y):
+                wy(j, h).wait_recv()
+                for i in range(1, C):
+                    wc(j, i, h).start()
+
+    def walk(s):
+        close_step(s)
+
+        @pl.when(s == Z - 2)
+        def _():
+            pass_weights()
+
+        is_end = jnp.logical_or(z == 0, z == Z - 1)
+        turn = jnp.where(is_end, 0, 1)
+
+        def one(t):
+            @pl.when(jnp.logical_and(t == turn, s + 1 < Z - 1))
+            def _():
+                open_step(s + 1)
+
+            d = inward(t)
+
+            @pl.when(gets(d, s))
+            def _():
+                plane = source(d, s + 1)
+                wait_across(1 + hop(d, s), plane)
+                attend(plane, False)
+
+        loop(0, 2, one)
+
+    if Z > 1:
+        open_step(0)
+    wait_across(0, z)
+    attend(z, True)
+    if Z > 1:
+        loop(0, Z - 1, walk)
     else:
-        attend_step(Z - 2)
+        pass_weights()
 
     for h in range(q_heads):
         head_out[:, h * head_dim:(h + 1) * head_dim] = (acc[h] / ls[h]).astype(jnp.bfloat16)
 
-    for j in range(Y):
-        for i in range(1, C):
-            wc(j, i).wait_recv()
+    for h in range(pieces):
+        for j in range(Y):
+            for i in range(1, C):
+                wc(j, i, h).wait_recv()
 
     width = wall.shape[1]
     tile = min(256, width)
@@ -299,25 +386,33 @@
 
     for j in range(1, X):
         kx(j).wait_send()
+        hx(0, z, j).wait_send()
         vx(0, z, j).wait_send()
-    for d in range(2):
-        for s in range(Z - 1):
+
+    def drain(s):
+        def one(d):
             @pl.when(sends(d, s))
-            def _(d=d, s=s):
+            def _():
                 vz(d, s).wait_send()
+                hz(d, s).wait_send()
                 for j in range(X):
                     kz(d, s, j).wait_send()
 
             @pl.when(gets(d, s))
-            def _(d=d, s=s):
-                plane = z - s - 1 if d == 0 else z + s + 1
+            def _():
                 for j in range(1, X):
-                    vx(1 + s + d * (Z - 1), plane, j).wait_send()
-    for j in range(1, Y):
-        wy(j).wait_send()
-    for j in range(Y):
-        for i in range(1, C):
-            wc(j, i).wait_send()
+                    hx(1 + hop(d, s), source(d, s + 1), j).wait_send()
+                    vx(1 + hop(d, s), source(d, s + 1), j).wait_send()
+
+        loop(0, 2, one)
+
+    loop(0, Z - 1, drain)
+    for h in range(pieces):
+        for j in range(1, Y):
+            wy(j, h).wait_send()
+        for j in range(Y):
+            for i in range(1, C):
+                wc(j, i, h).wait_send()
 
 
 def attention(query, keys, values, q_gain, k_gain, cosine, sine, resid, norm_gain, out_weight):
@@ -331,6 +426,7 @@
     dma = pltpu.SemaphoreType.DMA
     vmem = pl.BlockSpec(memory_space=pltpu.VMEM)
     hops = 2 * max(planes - 1, 1)
+    pieces = 4 if out_weight.shape[0] % 64 == 0 else 1
     full_kv = (sp_count * rows, keys.shape[1])
     return pl.pallas_call(
         functools.partial(attention_kernel, planes, lanes_x, outer_dp, inner_dp),
@@ -356,8 +452,10 @@
             dma((hops * lanes_x,)), dma((hops * lanes_x,)),
             dma((hops,)), dma((hops,)),
             dma(((hops + 1) * lanes_x,)), dma(((hops + 1) * lanes_x,)),
-            dma((outer_dp,)), dma((outer_dp,)),
-            dma((outer_dp * inner_dp,)), dma((outer_dp * inner_dp,)),
+            dma((hops,)), dma((hops,)),
+            dma(((hops + 1) * lanes_x,)), dma(((hops + 1) * lanes_x,)),
+            dma((outer_dp * pieces,)), dma((outer_dp * pieces,)),
+            dma((outer_dp * inner_dp * pieces,)), dma((outer_dp * inner_dp * pieces,)),
             dma((2,)),
         ],
         compiler_params=pltpu.CompilerParams(

time: 209 us -> 197 us (0.943)
  Pallas kernels: 202 us -> 190 us
    pallas_call x1, Pallas kernels: 79.6 us -> 67.3 us  [attention(): pl.pallas_call(functools.partial(attention_kernel, planes, lanes_x, outer...]
where the time goes in v3:
time: 197 us
  Pallas kernels  190 us (96%)
  other arithmetic  4.64 us (2%)
  local copies, waits for them, and re-layouts  2.3 us (1%)
    pallas_call x1, Pallas kernels, experts(): pl.pallas_call(functools.partial(experts_kernel, planes, lanes_x, slots),...  123 us
    pallas_call x1, Pallas kernels, attention(): pl.pallas_call(functools.partial(attention_kernel, planes, lanes_x, outer...  67.3 us

profile of v3, /device:TPU:0, one launch (start us, length us, event | category | flops | bytes accessed | tf_op | source)
XLA Modules:
  0.0 197.0 jit_solution(11861725949022443975)
XLA Ops:
  0.0 0.7 convert_bitcast_fusion
  0.7 1.3 maximum_bitcast_fusion.meta_ref
  2.0 1.0 fusion
  3.0 0.8 pad_maximum_fusion.1.sin_ref
  3.8 0.8 pad_maximum_fusion.cos_ref
  4.7 67.3 %gathered_attention.1 = (bf16[256,2048]{1,0:T(8,128)(2,1)}, bf16[256,2048]{1,0:T(8,128)(2,1)}) custom-call(bf16[256,2048]{1,0:T(8,128)(2,1)} %bitcast.20, bf16[256,512]{1,0:T(8,128)(2,1)} %bitcast.22, bf16[256,512]{1,0:T(8,128)(2,1)} %bitcast.23, f32[1,128]{1,0:T(1,128)} %bitcast.26, f32[1,128]{1,0:T(1,128)} %bitcast.27, ...), custom_call_target="tpu_custom_call" | custom-call | tf_op jit(solution)/shard_map/gathered_attention/pallas_call | solution.py:431
  72.0 122.7 %routed_experts.1 = bf16[256,2048]{1,0:T(8,128)(2,1)} custom-call(f32[4,256]{1,0:T(4,128)} %maximum_bitcast_fusion.meta_ref, bf16[256,2048]{1,0:T(8,128)(2,1)} %get-tuple-element.7.normed_ref, bf16[256,2048]{1,0:T(8,128)(2,1)} %get-tuple-element.8.upd_ref, bf16[2048,1024]{1,0:T(8,128)(2,1)} %bitcast.16, bf16[2048,1024]{1,0:T(8,128)(2,1)} %bitcast.17, ...), custom_call_target="tpu_custom_call" | custom-call | tf_op jit(solution)/shard_map/routed_experts/pallas_call | solution.py:965
  194.7 2.3 %copy.17 = bf16[1,256,2048]{2,1,0:T(8,128)(2,1)} copy(bf16[1,256,2048]{2,1,0:T(8,128)(2,1)} %bitcast.19) | data formatting | bytes 2097152
  (2 shorter events, 0.0 us)

commit v4 on v3

--- a/solution.py
+++ b/solution.py
@@ -24,21 +24,19 @@
 
 def turn_tables(places, head_dim):
     quarter = head_dim // 4
-    inverse = THETA ** (-jnp.arange(quarter, dtype=jnp.float32) / quarter)
-    row = (places // GRID_W).astype(jnp.float32)[:, None] * inverse[None, :]
-    col = (places % GRID_W).astype(jnp.float32)[:, None] * inverse[None, :]
-    cosine = jnp.concatenate([jnp.cos(row)] * 2 + [jnp.cos(col)] * 2, axis=-1)
-    sine = jnp.concatenate(
-        [-jnp.sin(row), jnp.sin(row), -jnp.sin(col), jnp.sin(col)], axis=-1
-    )
-    return cosine, sine
+    lane = jnp.arange(head_dim, dtype=jnp.int32)[None, :]
+    inverse = THETA ** (-(lane % quarter).astype(jnp.float32) / quarter)
+    row, col = places[:, None] // GRID_W, places[:, None] % GRID_W
+    angle = jnp.where(lane < 2 * quarter, row, col).astype(jnp.float32) * inverse
+    sign = jnp.where(lane % (2 * quarter) < quarter, -1.0, 1.0)
+    return jnp.cos(angle), jnp.sin(angle) * sign
 
 
 def attention_kernel(
     planes, lanes_x, outer_dp, inner_dp,
-    q_ref, k_ref, v_ref, qg_ref, kg_ref, cos_ref, sin_ref, resid_ref, ng_ref, w_ref,
+    q_hbm, k_ref, v_ref, qg_ref, kg_ref, cos_ref, sin_ref, resid_hbm, ng_ref, w_ref,
     upd_ref, normed_ref,
-    kall, vall, wall, qt, acc, mx, ls, head_out,
+    q_ref, resid_ref, kall, vall, wall, qt, acc, mx, ls, head_out,
     kx_s, kx_r, kz_s, kz_r, hz_s, hz_r, hx_s, hx_r, vz_s, vz_r, vx_s, vx_r,
     wy_s, wy_r, wc_s, wc_r, loc,
 ):
@@ -84,6 +82,10 @@
     v_own.start()
     w_own = pltpu.make_async_copy(w_ref, wall.at[wrows(dp)], loc.at[1])
     w_own.start()
+    q_own = pltpu.make_async_copy(q_hbm, q_ref, loc.at[2])
+    q_own.start()
+    resid_own = pltpu.make_async_copy(resid_hbm, resid_ref, loc.at[3])
+    resid_own.start()
 
     lane = lax.broadcasted_iota(jnp.int32, (rows, head_dim), 1)
     first = lane % (head_dim // 2) < head_dim // 4
@@ -215,6 +217,7 @@
         qt[h] = turned(q_ref[:, at], qg_ref[...])
         return carry
 
+    q_own.wait()
     lax.fori_loop(0, q_heads // 4, prepare_queries, 0)
     for j in range(1, X):
         kx(j).wait_recv()
@@ -361,6 +364,7 @@
             for i in range(1, C):
                 wc(j, i, h).wait_recv()
 
+    resid_own.wait()
     width = wall.shape[1]
     tile = min(256, width)
 
@@ -428,6 +432,7 @@
     hops = 2 * max(planes - 1, 1)
     pieces = 4 if out_weight.shape[0] % 64 == 0 else 1
     full_kv = (sp_count * rows, keys.shape[1])
+    hbm = pl.BlockSpec(memory_space=pl.ANY)
     return pl.pallas_call(
         functools.partial(attention_kernel, planes, lanes_x, outer_dp, inner_dp),
         name="gathered_attention",
@@ -435,11 +440,11 @@
             jax.ShapeDtypeStruct((rows, width), jnp.bfloat16),
             jax.ShapeDtypeStruct((rows, width), jnp.bfloat16),
         ),
-        in_specs=[vmem, vmem, pl.BlockSpec(memory_space=pl.ANY)]
-        + [vmem] * 6
-        + [pl.BlockSpec(memory_space=pl.ANY)],
+        in_specs=[hbm, vmem, hbm] + [vmem] * 4 + [hbm, vmem, hbm],
         out_specs=(vmem, vmem),
         scratch_shapes=[
+            pltpu.VMEM(query.shape, jnp.bfloat16),
+            pltpu.VMEM(resid.shape, jnp.bfloat16),
             pltpu.VMEM(full_kv, jnp.bfloat16),
             pltpu.VMEM(full_kv, jnp.bfloat16),
             pltpu.VMEM((dp_count * out_weight.shape[0], width), jnp.bfloat16),
@@ -456,7 +461,7 @@
             dma(((hops + 1) * lanes_x,)), dma(((hops + 1) * lanes_x,)),
             dma((outer_dp * pieces,)), dma((outer_dp * pieces,)),
             dma((outer_dp * inner_dp * pieces,)), dma((outer_dp * inner_dp * pieces,)),
-            dma((2,)),
+            dma((4,)),
         ],
         compiler_params=pltpu.CompilerParams(
             collective_id=0, has_side_effects=True, vmem_limit_bytes=VMEM_BYTES
@@ -469,9 +474,9 @@
 
 def experts_kernel(
     planes, lanes_x, slots,
-    meta_ref, normed_ref, upd_ref, gate_hbm, up_hbm, down_hbm,
+    ids_ref, scale_ref, normed_ref, upd_hbm, gate_hbm, up_hbm, down_hbm,
     out_ref,
-    meta, raw, pk, epk, xb, rb, fr, fp, ptab, whi, wlo, tri, xs, act, acc, gate_w, up_w, down_w,
+    meta, upd_ref, raw, pk, epk, xb, rb, fr, fp, ptab, whi, wlo, tri, xs, sums, act, acc, gate_w, up_w, down_w,
     meta_s, meta_r, zs, zr, es, er, rs, rr, fs, fa, loc,
 ):
     Z, X, K = planes, lanes_x, slots
@@ -479,7 +484,7 @@
     DP = lax.axis_size("dp")
     EP = X * DP
     S = EP * K
-    top = meta_ref.shape[0] // 2
+    top = ids_ref.shape[0]
     chunks = zr.shape[1]
     part = width // chunks
     hidden = gate_w.shape[1]
@@ -522,6 +527,10 @@
         greet((((z + j) % Z) * X + x, dp))
     for copy in weights:
         copy.start()
+    upd_copy = pltpu.make_async_copy(upd_hbm, upd_ref, loc.at[3])
+    upd_copy.start()
+    meta[z, :top] = ids_ref[...].astype(f32)
+    meta[z, top:] = scale_ref[...]
     tri[...] = (
         lax.broadcasted_iota(jnp.int32, (rows, rows), 0)
         < lax.broadcasted_iota(jnp.int32, (rows, rows), 1)
@@ -551,7 +560,7 @@
 
     def meta_copy(j):
         return remote(
-            meta_ref, meta.at[z], meta_s.at[j], meta_r.at[z], (((z + j) % Z) * X + x, dp)
+            meta.at[z], meta.at[z], meta_s.at[j], meta_r.at[z], (((z + j) % Z) * X + x, dp)
         )
 
     def own_raw(d, ck):
@@ -651,7 +660,6 @@
             loop(0, chunks, lambda ck: own_raw(d, ck).start())
 
     loop(0, 2, own_raw_start)
-    meta[z] = meta_ref[...]
 
     def own_packed(d, low, high):
         @pl.when(jnp.logical_and(exists(d), next_end(d)))
@@ -683,6 +691,10 @@
 
     loop(0, chunks, own_chunk)
 
+    def held(src, ck):
+        near = jnp.logical_or(src == z + 1, src == z - 1)
+        return jnp.logical_and(near, ck >= early) if Z > 2 else False
+
     def carry_on(d, src, ck):
         @pl.when(ck == 0)
         def _():
@@ -691,7 +703,10 @@
         @pl.when(at_end(d))
         def _():
             landed(pk, (src, slice(None), slice(None), cols(ck)), zr.at[src, ck])
-            spread(src, ck)
+
+            @pl.when(jnp.logical_not(held(src, ck)))
+            def _():
+                spread(src, ck)
 
         @pl.when(jnp.logical_not(at_end(d)))
         def _():
@@ -724,18 +739,34 @@
             landed(xb, (src, slice(None), slice(None), cols(ck)), er.at[src, ck])
             xs[:, cols(ck)] = xb[src, :, :, cols(ck)].reshape(S, part)
 
-        loop(0, chunks, gather)
+        def products(at, low, high):
+            span = slice(low * part, high * part)
+            return [
+                jnp.dot(xs[:, span], matrix[span, at], preferred_element_type=f32)
+                for matrix in (gate_w, up_w)
+            ]
+
+        def spot(n):
+            return pl.ds(pl.multiple_of(n * tile, tile), tile)
+
+        def begin(n):
+            for i, value in enumerate(products(spot(n), 0, chunks - 1)):
+                sums[i, :, spot(n)] = value
 
         def inner(n):
-            at = pl.ds(pl.multiple_of(n * tile, tile), tile)
-            gated = jnp.minimum(
-                jnp.dot(xs[...], gate_w[:, at], preferred_element_type=f32), LIMIT
-            )
-            linear = jnp.clip(
-                jnp.dot(xs[...], up_w[:, at], preferred_element_type=f32), -LIMIT, LIMIT
-            )
-            act[:, at] = (gated * jax.nn.sigmoid(SLOPE * gated) * (linear + 1.0)).astype(bf16)
-
+            values = products(spot(n), chunks - 1 if chunks > 1 else 0, chunks)
+            if chunks > 1:
+                values = [value + sums[i, :, spot(n)] for i, value in enumerate(values)]
+            gated = jnp.minimum(values[0], LIMIT)
+            linear = jnp.clip(values[1], -LIMIT, LIMIT)
+            act[:, spot(n)] = (
+                gated * jax.nn.sigmoid(SLOPE * gated) * (linear + 1.0)
+            ).astype(bf16)
+
+        if chunks > 1:
+            loop(0, chunks - 1, gather)
+            loop(0, hidden // tile, begin)
+        gather(chunks - 1)
         loop(0, hidden // tile, inner)
 
         def outer(ck):
@@ -799,19 +830,20 @@
         for copy in weights:
             copy.wait()
 
-    def backward(k):
-        def chunk(ck):
+    def backward(k, low, high):
+        def turn(i):
             def one(t):
-                d = jnp.where(2 * z >= Z, t, 1 - t)
+                d, ck = inward(t), i - t
                 src = (Z - 1 - k) * (1 - d) + k * d
-
-                @pl.when((z - src) * toward(d) > 0)
+                ready = jnp.logical_and(ck >= low, ck < high)
+
+                @pl.when(jnp.logical_and(ready, (z - src) * toward(d) > 0))
                 def _():
                     send_back(d, src, ck)
 
             loop(0, 2, one)
 
-        loop(0, chunks, chunk)
+        loop(low, high + 1, turn)
 
     def away(s):
         if Z < 3:
@@ -850,6 +882,12 @@
             late_end = jnp.logical_and(is_end, s == 3)
             first = jnp.where(is_end, min(1, last), 0)
 
+            lead = jnp.logical_and(jnp.logical_and(s > 2, s < Z), ck == 0)
+
+            @pl.when(jnp.logical_and(lead, jnp.logical_not(is_end)))
+            def _():
+                backward(s - 1, 0, 1)
+
             @pl.when(jnp.logical_and(jnp.logical_and(s > 1, ck == first), jnp.logical_not(late_end)))
             def _():
                 expert(away(s - 1), 0, True)
@@ -865,6 +903,12 @@
                     loop(0, 2, lambda d: own_packed(d, early, chunks))
                     run_expert(z, False)
 
+                if Z > 2:
+                    @pl.when(jnp.logical_and(is_end, s == Z - 1))
+                    def _():
+                        beside = jnp.where(z == 0, 1, Z - 2)
+                        loop(early, chunks, lambda i: spread(beside, i))
+
                 src = z - (s - 1) * toward(inward(1))
 
                 @pl.when(jnp.logical_and(middle, within(src)))
@@ -873,23 +917,27 @@
 
                 @pl.when(s == Z)
                 def _():
-                    if Z > 2:
-                        @pl.when(is_end)
-                        def _():
-                            expert(away(2), 0, True)
                     loop(0, chunks, lambda i: give_back(z, i))
 
+            ahead = jnp.where(s < Z, 1, 0)
             turn = jnp.where(jnp.logical_and(is_end, s < Z), 0, last)
 
             @pl.when(jnp.logical_and(s > 2, ck == turn))
             def _():
-                backward(s - 1)
+                backward(s - 1, jnp.where(is_end, 0, ahead), chunks)
+
+            if Z > 2:
+                @pl.when(jnp.logical_and(jnp.logical_and(s == Z, ck == last), is_end))
+                def _():
+                    expert(away(2), 0, True)
 
         loop(0, chunks, chunk)
 
     loop(1, Z + 1, stage)
     if Z > 1:
-        backward(1)
+        backward(1, 0, chunks)
+
+    upd_copy.wait()
 
     def finish(ck):
         returned(z, ck)
@@ -957,7 +1005,6 @@
     padded = -(-group * slots // 128) * 128
     hidden = gate_matrix.shape[1]
     chunks = CHUNKS if width % (128 * CHUNKS) == 0 else 1
-    meta = jnp.concatenate([route_ids.astype(jnp.float32), route_weight], axis=1).T
     dma = pltpu.SemaphoreType.DMA
     vmem = pl.BlockSpec(memory_space=pltpu.VMEM)
     hbm = pl.BlockSpec(memory_space=pl.ANY)
@@ -966,10 +1013,11 @@
         functools.partial(experts_kernel, planes, lanes_x, slots),
         name="routed_experts",
         out_shape=jax.ShapeDtypeStruct((rows, width), bf16),
-        in_specs=[vmem] * 3 + [hbm] * 3,
+        in_specs=[vmem] * 3 + [hbm] * 4,
         out_specs=vmem,
         scratch_shapes=[
             pltpu.VMEM((planes, 2 * top, rows), f32),
+            pltpu.VMEM((rows, width), bf16),
             pltpu.VMEM((planes, rows, width), bf16),
             pltpu.VMEM((planes, group, slots, width), bf16),
             pltpu.VMEM((planes + 1, group, slots, width), bf16),
@@ -982,6 +1030,7 @@
             pltpu.VMEM((2 * planes + 1, rows, padded), bf16),
             pltpu.VMEM((rows, rows), bf16),
             pltpu.VMEM((group * slots, width), bf16),
+            pltpu.VMEM((2, group * slots, hidden), f32),
             pltpu.VMEM((group * slots, hidden), bf16),
             pltpu.VMEM((rows, width // chunks), f32),
             pltpu.VMEM(gate_matrix.shape, bf16),
@@ -992,12 +1041,12 @@
             dma((planes, chunks)), dma((planes, chunks)),
             dma((planes, chunks)), dma((planes, chunks)),
             dma((planes, chunks)), dma((planes + 1, chunks)),
-            dma((3,)),
+            dma((4,)),
         ],
         compiler_params=pltpu.CompilerParams(
             collective_id=1, has_side_effects=True, vmem_limit_bytes=VMEM_BYTES
         ),
-    )(meta, normed, updated, gate_matrix, up_matrix, down_matrix)
+    )(route_ids.T, route_weight.T, normed, updated, gate_matrix, up_matrix, down_matrix)
 
 
 def per_device(

time: 197 us -> 186 us (0.944)
  Pallas kernels: 190 us -> 182 us
  other arithmetic: 4.64 us -> 1.28 us
    pallas_call x1, Pallas kernels: 123 us -> 115 us  [experts(): pl.pallas_call(functools.partial(experts_kernel, planes, lanes_x, slots),...]
where the time goes in v4:
time: 186 us
  Pallas kernels  182 us (98%)
  local copies, waits for them, and re-layouts  2.3 us (1%)
    pallas_call x1, Pallas kernels, experts(): pl.pallas_call(functools.partial(experts_kernel, planes, lanes_x, slots),...  115 us
    pallas_call x1, Pallas kernels, attention(): pl.pallas_call(functools.partial(attention_kernel, planes, lanes_x, outer...  66.7 us

profile of v4, /device:TPU:0, one launch (start us, length us, event | category | flops | bytes accessed | tf_op | source)
XLA Modules:
  0.0 185.6 jit_solution(16971412980337983590)
XLA Ops:
  0.0 1.3 sine_multiply_fusion
  1.3 66.7 %gathered_attention.1 = (bf16[256,2048]{1,0:T(8,128)(2,1)}, bf16[256,2048]{1,0:T(8,128)(2,1)}) custom-call(bf16[256,2048]{1,0:T(8,128)(2,1)} %bitcast.21, bf16[256,512]{1,0:T(8,128)(2,1)} %bitcast.23, bf16[256,512]{1,0:T(8,128)(2,1)} %bitcast.24, f32[1,128]{1,0:T(1,128)} %bitcast.28, f32[1,128]{1,0:T(1,128)} %bitcast.29, ...), custom_call_target="tpu_custom_call" | custom-call | tf_op jit(solution)/shard_map/gathered_attention/pallas_call | solution.py:436
  68.0 115.3 %routed_experts.1 = bf16[256,2048]{1,0:T(8,128)(2,1)} custom-call(s32[2,256]{1,0:T(2,128)} %bitcast.26, f32[2,256]{1,0:T(2,128)} %bitcast.27, bf16[256,2048]{1,0:T(8,128)(2,1)} %get-tuple-element.7.normed_ref, bf16[256,2048]{1,0:T(8,128)(2,1)} %get-tuple-element.8.upd_hbm, bf16[2048,1024]{1,0:T(8,128)(2,1)} %bitcast.17, bf16[2048,1024]{1,0:T(8,128)(2,1)} %bitcast.18, ...), custom_call_target="tpu_custom_call" | custom-call | tf_op jit(solution)/shard_map/routed_experts/pallas_call | solution.py:1012
  183.3 2.3 %copy.15 = bf16[1,256,2048]{2,1,0:T(8,128)(2,1)} copy(bf16[1,256,2048]{2,1,0:T(8,128)(2,1)} %bitcast.20) | data formatting | bytes 2097152
  (3 shorter events, 0.0 us)

commit v5 on v4

--- a/solution.py
+++ b/solution.py
@@ -231,7 +231,7 @@
     factor = head_dim ** (-0.5) * LOG2E
     keys_in = X * rows
 
-    def attend(plane, fresh):
+    def attend(plane, fresh, begin, end):
         at_rows = pl.ds(pl.multiple_of(plane * keys_in, keys_in), keys_in)
 
         def one_group(i, carry):
@@ -263,7 +263,7 @@
                 mx[h] = wide
             return carry
 
-        lax.fori_loop(0, kv_heads, one_group, 0)
+        lax.fori_loop(begin, end, one_group, 0)
 
     def wait_across(slot, plane):
         for j in range(1, X):
@@ -325,11 +325,14 @@
     def walk(s):
         close_step(s)
 
-        @pl.when(s == Z - 2)
+        is_end = jnp.logical_or(z == 0, z == Z - 1)
+        final = s == Z - 2
+
+        @pl.when(jnp.logical_and(final, jnp.logical_not(is_end)))
         def _():
             pass_weights()
 
-        is_end = jnp.logical_or(z == 0, z == Z - 1)
+        middle = max(kv_heads // 2, 1)
         turn = jnp.where(is_end, 0, 1)
 
         def one(t):
@@ -343,14 +346,22 @@
             def _():
                 plane = source(d, s + 1)
                 wait_across(1 + hop(d, s), plane)
-                attend(plane, False)
+
+                def part(u):
+                    attend(plane, False, u * middle, jnp.where(u == 0, middle, kv_heads))
+
+                    @pl.when(jnp.logical_and(jnp.logical_and(final, is_end), u == 0))
+                    def _():
+                        pass_weights()
+
+                loop(0, 2, part)
 
         loop(0, 2, one)
 
     if Z > 1:
         open_step(0)
     wait_across(0, z)
-    attend(z, True)
+    attend(z, True, 0, kv_heads)
     if Z > 1:
         loop(0, Z - 1, walk)
     else:
@@ -702,10 +713,9 @@
 
         @pl.when(at_end(d))
         def _():
-            landed(pk, (src, slice(None), slice(None), cols(ck)), zr.at[src, ck])
-
             @pl.when(jnp.logical_not(held(src, ck)))
             def _():
+                landed(pk, (src, slice(None), slice(None), cols(ck)), zr.at[src, ck])
                 spread(src, ck)
 
         @pl.when(jnp.logical_not(at_end(d)))
@@ -856,6 +866,8 @@
     def within(src):
         return jnp.logical_and(src >= 0, src < Z)
 
+    lead = min(2, chunks)
+
     def stage(s):
         def chunk(ck):
             def one(d):
@@ -865,6 +877,12 @@
                 def _():
                     carry_on(d, src, ck)
 
+            each = jnp.logical_and(is_end, jnp.logical_and(s > 2, s < Z))
+
+            @pl.when(each)
+            def _():
+                backward(s - 1, ck, ck + 1)
+
             loop(0, 2, one)
 
             @pl.when(jnp.logical_and(s == 1, ck == 0))
@@ -882,11 +900,11 @@
             late_end = jnp.logical_and(is_end, s == 3)
             first = jnp.where(is_end, min(1, last), 0)
 
-            lead = jnp.logical_and(jnp.logical_and(s > 2, s < Z), ck == 0)
-
-            @pl.when(jnp.logical_and(lead, jnp.logical_not(is_end)))
-            def _():
-                backward(s - 1, 0, 1)
+            before = jnp.logical_and(jnp.logical_and(s > 2, s < Z), ck == 0)
+
+            @pl.when(jnp.logical_and(before, jnp.logical_not(is_end)))
+            def _():
+                backward(s - 1, 0, lead)
 
             @pl.when(jnp.logical_and(jnp.logical_and(s > 1, ck == first), jnp.logical_not(late_end)))
             def _():
@@ -895,19 +913,27 @@
             @pl.when(jnp.logical_and(middle, ck == min(1, last)))
             def _():
                 expert(s - 1, 1, False)
+
+            own_turn = jnp.where(is_end, min(1, last), last)
 
             @pl.when(ck == last)
             def _():
                 @pl.when(s == 1)
                 def _():
                     loop(0, 2, lambda d: own_packed(d, early, chunks))
-                    run_expert(z, False)
 
                 if Z > 2:
                     @pl.when(jnp.logical_and(is_end, s == Z - 1))
                     def _():
                         beside = jnp.where(z == 0, 1, Z - 2)
-                        loop(early, chunks, lambda i: spread(beside, i))
+
+                        def late(i):
+                            landed(
+                                pk, (beside, slice(None), slice(None), cols(i)), zr.at[beside, i]
+                            )
+                            spread(beside, i)
+
+                        loop(early, chunks, late)
 
                 src = z - (s - 1) * toward(inward(1))
 
@@ -919,12 +945,15 @@
                 def _():
                     loop(0, chunks, lambda i: give_back(z, i))
 
-            ahead = jnp.where(s < Z, 1, 0)
-            turn = jnp.where(jnp.logical_and(is_end, s < Z), 0, last)
-
-            @pl.when(jnp.logical_and(s > 2, ck == turn))
-            def _():
-                backward(s - 1, jnp.where(is_end, 0, ahead), chunks)
+            @pl.when(jnp.logical_and(s == 1, ck == own_turn))
+            def _():
+                run_expert(z, False)
+
+            turn = jnp.logical_or(s == Z, jnp.logical_not(is_end))
+
+            @pl.when(jnp.logical_and(jnp.logical_and(s > 2, ck == last), turn))
+            def _():
+                backward(s - 1, jnp.where(s < Z, lead, 0), chunks)
 
             if Z > 2:
                 @pl.when(jnp.logical_and(jnp.logical_and(s == Z, ck == last), is_end))

time: 186 us -> 181 us (0.973)
  Pallas kernels: 182 us -> 177 us
    pallas_call x1, Pallas kernels: 115 us -> 110 us  [experts(): pl.pallas_call(functools.partial(experts_kernel, planes, lanes_x, slots),...]
where the time goes in v5:
time: 181 us
  Pallas kernels  177 us (98%)
  local copies, waits for them, and re-layouts  2.3 us (1%)
    pallas_call x1, Pallas kernels, experts(): pl.pallas_call(functools.partial(experts_kernel, planes, lanes_x, slots),...  110 us
    pallas_call x1, Pallas kernels, attention(): pl.pallas_call(functools.partial(attention_kernel, planes, lanes_x, outer...  66.6 us

profile of v5, /device:TPU:0, one launch (start us, length us, event | category | flops | bytes accessed | tf_op | source)
XLA Modules:
  0.0 180.7 jit_solution(14259418309922401750)
XLA Ops:
  0.0 1.3 sine_multiply_fusion
  1.3 66.6 %gathered_attention.1 = (bf16[256,2048]{1,0:T(8,128)(2,1)}, bf16[256,2048]{1,0:T(8,128)(2,1)}) custom-call(bf16[256,2048]{1,0:T(8,128)(2,1)} %bitcast.21, bf16[256,512]{1,0:T(8,128)(2,1)} %bitcast.23, bf16[256,512]{1,0:T(8,128)(2,1)} %bitcast.24, f32[1,128]{1,0:T(1,128)} %bitcast.28, f32[1,128]{1,0:T(1,128)} %bitcast.29, ...), custom_call_target="tpu_custom_call" | custom-call | tf_op jit(solution)/shard_map/gathered_attention/pallas_call | solution.py:447
  67.9 110.5 %routed_experts.1 = bf16[256,2048]{1,0:T(8,128)(2,1)} custom-call(s32[2,256]{1,0:T(2,128)} %bitcast.26, f32[2,256]{1,0:T(2,128)} %bitcast.27, bf16[256,2048]{1,0:T(8,128)(2,1)} %get-tuple-element.7.normed_ref, bf16[256,2048]{1,0:T(8,128)(2,1)} %get-tuple-element.8.upd_hbm, bf16[2048,1024]{1,0:T(8,128)(2,1)} %bitcast.17, bf16[2048,1024]{1,0:T(8,128)(2,1)} %bitcast.18, ...), custom_call_target="tpu_custom_call" | custom-call | tf_op jit(solution)/shard_map/routed_experts/pallas_call | solution.py:1041
  178.4 2.3 %copy.15 = bf16[1,256,2048]{2,1,0:T(8,128)(2,1)} copy(bf16[1,256,2048]{2,1,0:T(8,128)(2,1)} %bitcast.20) | data formatting | bytes 2097152
  (3 shorter events, 0.0 us)
